TPU v7x, 32 devices: a whole 2x2x4 slice. The times are simulated.
32 devices in a mesh: sp: 16 (over z, y, core), tp: 2 (over x).
Axes of the slice: x: 2, y: 2, z: 4, core: 2. Of those that a mesh axis runs over, the one named last changes fastest.
Arguments:
- glu_value: bfloat16 [8192, 1024], P('sp', 'tp'), may hold values from -6 to 6
- glu_gate: bfloat16 [8192, 1024], P('sp', 'tp'), may hold values from -8 to 8
- conv_taps: float32 [31, 1024], P(None, 'tp'), may hold values from -1 to 1
- channel_norm_gain: float32 [1024], P('tp'), may hold values from 0.1 to 1.9
- channel_norm_bias: float32 [1024], P('tp'), may hold values from -3 to 3
- out_proj: bfloat16 [1024, 2048], P('tp'), may hold values from -0.1875 to 0.1875
- out_grad: bfloat16 [8192, 2048], P('sp'), may hold values from -6 to 6
Outputs:
- grad_value: bfloat16 [8192, 1024], P('sp', 'tp')
- grad_gate: bfloat16 [8192, 1024], P('sp', 'tp')
- grad_taps: float32 [31, 1024], P(None, 'tp')
- norm_gain_gradient: float32 [1024], P('tp')
- grad_bias: float32 [1024], P('tp')
- grad_proj: float32 [2048, 1024], P('sp', 'tp')
All inputs are finite; a program needn't handle non-finite values.
Results may differ from a plain program's by a relative error of at most 0.0049.
Values may be sent and summed in bfloat16 or wider, within the bound.
No kernel may reach another device: no remote copies, remote signals or barrier semaphores. Data moves between devices by JAX's collectives and lax.ppermute only.
A program may use at most 64 MiB of HBM per device.

v0:
```python
import jax
import jax.numpy as jnp
from jax import lax
from jax.sharding import PartitionSpec as P

CONV_CHANNELS = 1024
TAPS = 31


def passed_along(shard, axis, by):
    size = lax.axis_size(axis)
    pairs = [(i, i + by) for i in range(size) if 0 <= i + by < size]
    return lax.ppermute(shard, axis, pairs)


def on_device(
    glu_value, glu_gate, conv_taps, channel_norm_gain, channel_norm_bias, out_proj, out_grad
):
    rows, width = glu_value.shape
    value = glu_value.astype(jnp.float32)
    sig_gate = jax.nn.sigmoid(glu_gate.astype(jnp.float32))
    gated = (value * sig_gate).astype(jnp.bfloat16)
    before = passed_along(gated[rows - (TAPS - 1) :], "sp", 1)
    padded = jnp.concatenate([before, gated], axis=0).astype(jnp.float32)
    conv_output = jnp.zeros((rows, width), jnp.float32)
    for k in range(TAPS):
        conv_output = conv_output + conv_taps[k][None, :] * padded[k : k + rows]
    total, squares = lax.psum(
        (jnp.sum(conv_output, axis=1), jnp.sum(conv_output * conv_output, axis=1)), "tp"
    )
    channel_mean = (total / CONV_CHANNELS)[:, None]
    var = (squares / CONV_CHANNELS)[:, None] - channel_mean * channel_mean
    inverse_deviation = lax.rsqrt(var + 1e-05)
    centered_standardized = (conv_output - channel_mean) * inverse_deviation
    normalized_rows = (
        centered_standardized * channel_norm_gain[None, :] + channel_norm_bias[None, :]
    )
    sig_norm = jax.nn.sigmoid(normalized_rows)
    act = (normalized_rows * sig_norm).astype(jnp.bfloat16)
    grad_act = lax.dot_general(
        out_grad, out_proj, (((1,), (1,)), ((), ())), preferred_element_type=jnp.float32
    )
    grad_proj = lax.psum_scatter(
        lax.dot_general(
            out_grad, act, (((0,), (0,)), ((), ())), preferred_element_type=jnp.float32
        ),
        "sp",
        scatter_dimension=0,
        tiled=True,
    )
    normalized_gradient = grad_act * sig_norm * (1.0 + normalized_rows * (1.0 - sig_norm))
    scaled_rows = normalized_gradient * channel_norm_gain[None, :]
    first_term, second_term = lax.psum(
        (jnp.sum(scaled_rows, axis=1), jnp.sum(scaled_rows * centered_standardized, axis=1)), "tp"
    )
    conv_output_gradient = inverse_deviation * (
        scaled_rows
        - (first_term / CONV_CHANNELS)[:, None]
        - centered_standardized * (second_term / CONV_CHANNELS)[:, None]
    )
    taps_local = jnp.stack(
        [jnp.sum(conv_output_gradient * padded[k : k + rows], axis=0) for k in range(TAPS)], axis=0
    )
    packed = jnp.concatenate(
        [
            taps_local,
            jnp.sum(normalized_gradient * centered_standardized, axis=0)[None, :],
            jnp.sum(normalized_gradient, axis=0)[None, :],
        ],
        axis=0,
    )
    share = lax.psum_scatter(packed, "sp", scatter_dimension=1, tiled=True)
    summed = lax.all_gather(share, "sp", axis=1, tiled=True)
    ahead = passed_along(conv_output_gradient[: TAPS - 1], "sp", -1)
    after = jnp.concatenate([conv_output_gradient, ahead], axis=0)
    grad_gated = jnp.zeros((rows, width), jnp.float32)
    for k in range(TAPS):
        grad_gated = grad_gated + conv_taps[k][None, :] * after[TAPS - 1 - k : TAPS - 1 - k + rows]
    grad_value = (grad_gated * sig_gate).astype(jnp.bfloat16)
    grad_gate = (grad_gated * value * sig_gate * (1.0 - sig_gate)).astype(jnp.bfloat16)
    return (grad_value, grad_gate, summed[:TAPS], summed[TAPS], summed[TAPS + 1], grad_proj)


def solution(mesh):
    return jax.shard_map(
        on_device,
        mesh=mesh,
        in_specs=(
            P("sp", "tp"),
            P("sp", "tp"),
            P(None, "tp"),
            P("tp"),
            P("tp"),
            P("tp", None),
            P("sp", None),
        ),
        out_specs=(P("sp", "tp"), P("sp", "tp"), P(None, "tp"), P("tp"), P("tp"), P("sp", "tp")),
        check_vma=False,
    )
```

profile of v0, /device:TPU:0, one launch (start us, length us, event | category | flops | bytes accessed | tf_op | source)
XLA Modules:
  0.0 184.4 jit_solution(906869488730801096)
XLA Ops:
  7.2 0.0 copy-start
  7.2 0.0 reduce-scatter.7.cloned.1.call-start
  7.2 1.6 fusion.1
  8.9 2.4 %collective-permute-start = (bf16[30,512]{1,0:T(8,128)(2,1)S(1)}, bf16[30,512]{1,0:T(8,128)(2,1)S(1)}, u32[]{:S(2)}, u32[]{:S(2)}) collective-permute-start(bf16[30,512]{1,0:T(8,128)(2,1)S(1)} %slice.450), channel_id=1, source_target_pairs={{0,2},{2,4},{4,6},{6,8},{8,10},{10,12},{12,14},{14,16},{16,18},{18... | collective-permute-start | bytes 92168 | tf_op jit(solution)/shard_map/ppermute | solution.py:13
  11.3 1.1 fusion.101
  12.4 1.0 fusion.102
  13.5 0.0 collective-permute-done
  13.5 0.2 maximum_convert_fusion
  13.6 0.0 copy-start.4
  13.6 0.0 copy-start.5
  13.7 5.7 %multiply_reduce_fusion.33 = (f32[512]{0:T(512)S(1)}, f32[512]{0:T(512)S(1)}, f32[512,512]{1,0:T(8,128)}) fusion(f32[542,512]{1,0:T(8,128)S(1)} %maximum_convert_fusion, f32[512]{0:T(512)S(1)} %bitcast.132, f32[512]{0:T(512)S(1)} %bitcast.134, f32[512]{0:T(512)S(1)} %bitcast.76, f32[512]{0:T(512)S(1)} %bitcast.78, f32[512]{0:T(512)S(1)} %bitcast.80, ...), kind=kLoop, calls=%fused_computation.184 | loop fusion | flops 16776192 | bytes 33622016 | tf_op jit(solution)/shard_map/reduce_sum | solution.py:29
  19.4 5.2 %all-reduce.1 = (f32[512]{0:T(512)S(1)}, f32[512]{0:T(512)S(1)}) all-reduce(f32[512]{0:T(512)S(1)} %get-tuple-element.60, f32[512]{0:T(512)S(1)} %get-tuple-element.59), channel_id=1, replica_groups=mesh['sp'=16,'tp'=2] {'tp'}, use_global_device_ids=true, to_apply=%region_3.0 | all-reduce | flops 1024 | bytes 8192 | tf_op jit(solution)/shard_map/psum | solution.py:28
  24.6 0.0 copy-done
  24.6 0.0 copy-done.4
  24.6 0.0 copy-done.5
  24.6 4.6 %multiply_reduce_fusion = (f32[512]{0:T(512)S(1)}, f32[512]{0:T(512)S(1)}, f32[512]{0:T(512)S(1)}, f32[512]{0:T(512)S(1)}, f32[512,512]{1,0:T(8,128)}) fusion(f32[512,512]{1,0:T(8,128)} %get-tuple-element.70, f32[512]{0:T(512)S(1)} %get-tuple-element.103, f32[512]{0:T(512)S(1)} %get-tuple-element.102, f32[512]{0:T(512)S(1)} %copy-done.4, ...), kind=kOutput, calls=%fused_computation.146 | convolution fusion | flops 1078720512 | bytes 6307840 | tf_op jit(solution)/shard_map/dot_general | solution.py:40
  29.2 4.9 %all-reduce = (f32[512]{0:T(512)S(1)}, f32[512]{0:T(512)S(1)}) all-reduce(f32[512]{0:T(512)S(1)} %get-tuple-element.56, f32[512]{0:T(512)S(1)} %get-tuple-element.57), channel_id=1, replica_groups=mesh['sp'=16,'tp'=2] {'tp'}, use_global_device_ids=true, to_apply=%region_7.0 | all-reduce | flops 1024 | bytes 8192 | tf_op jit(solution)/shard_map/psum | solution.py:53
  34.1 4.2 %multiply_reduce_fusion.1 = (f32[512]{0:T(512)S(1)}, f32[512]{0:T(512)S(1)}, f32[512]{0:T(512)S(1)}, f32[512]{0:T(512)S(1)}, f32[512]{0:T(512)S(1)}, /*index=5*/...) fusion(f32[542,512]{1,0:T(8,128)S(1)} %maximum_convert_fusion, ...), kind=kLoop, calls=%fused_computation.147 | loop fusion | flops 11262976 | bytes 22067200 | tf_op jit(solution)/shard_map/reduce_sum | solution.py:62
  38.3 0.0 copy-start.1
  38.3 1.7 multiply_reduce_fusion.19
  40.0 0.0 copy-done.1
  40.0 0.2 concatenate.11
  40.2 0.8 copy.20
  41.0 0.0 reduce-scatter.7.cloned.1.call-update
  41.1 0.0 reduce-scatter.5.cloned.1.call-start
  41.1 4.6 %convolution_bitcast_fusion = f32[2048,512]{0,1:T(8,128)} fusion(bf16[512,2048]{1,0:T(8,128)(2,1)S(1)} %copy-done, f32[512,512]{1,0:T(8,128)} %get-tuple-element.70, f32[512]{0:T(512)S(1)} %copy-done.5, f32[512]{0:T(512)S(1)} %copy-done.4, f32[512]{0:T(512)S(1)} %get-tuple-element.103, f32[512]{0:T(512)S(1)} %get-tuple-element.102), kind=kOutput, calls=%fused_computation.29 | convolution fusion | flops 1076101120 | bytes 7348224 | tf_op jit(solution)/shard_map/dot_general | solution.py:44
  45.7 0.0 copy-start.2
  45.7 0.0 reduce-scatter.5.cloned.1.call-update
  45.8 1.2 copy-done.2
  47.0 0.0 copy-start.3
  47.0 1.4 collective-permute-start.1
  48.4 1.8 %collective-permute-done.1 = f32[30,512]{1,0:T(8,128)S(1)} collective-permute-done((f32[30,512]{1,0:T(8,128)S(1)}, f32[30,512]{1,0:T(8,128)S(1)}, u32[]{:S(2)}, u32[]{:S(2)}) %collective-permute-start.1) | collective-permute-done | bytes 61472 | tf_op jit(solution)/shard_map/ppermute | solution.py:13
  50.2 7.0 %fusion.4 = (bf16[512,512]{1,0:T(8,128)(2,1)}, f32[512,512]{1,0:T(8,128)S(1)}) fusion(bf16[512,512]{1,0:T(8,128)(2,1)} %param.7, bf16[512,512]{1,0:T(8,128)(2,1)} %param.8, f32[512,512]{1,0:T(8,128)S(1)} %copy-done.2, f32[512]{0:T(512)S(1)} %bitcast.133, f32[30,512]{1,0:T(8,128)S(1)} %collective-permute-done.1, f32[512]{0:T(512)S(1)} %bitcast.135, ...), kind=kLoop, calls=%fused_computation.37 | loop fusion | flops 26476544 | bytes 3794944 | tf_op jit(solution)/shard_map/convert_element_type | solution.py:80
  57.2 0.0 copy-done.3
  57.2 1.1 multiply_convert_fusion.1
  58.3 41.8 %reduce-scatter.7.cloned.1.call-done = f32[32,33]{1,0:T(8,128)} async-done(((f32[512,33]{1,0:T(8,128)}), f32[32,33]{1,0:T(8,128)}) %reduce-scatter.7.cloned.1.call-update) | async-done | bytes 4240
  100.1 20.3 %all_gather.3 = f32[33,512]{0,1:T(8,128)S(1)} all-gather(f32[33,32]{0,1:T(8,128)} %bitcast.136), channel_id=1, replica_groups=mesh['sp'=16,'tp'=2] {'sp'}, dimensions={1}, use_global_device_ids=true | all-gather | bytes 71808 | tf_op jit(solution)/shard_map/all_gather | solution.py:73
  120.4 0.7 copy.18
  121.2 1.0 slice_reduce_fusion
  122.1 53.6 %reduce-scatter.5.cloned.1.call-done = f32[128,512]{0,1:T(8,128)} async-done(((f32[2048,512]{0,1:T(8,128)}), f32[128,512]{0,1:T(8,128)}) %reduce-scatter.5.cloned.1.call-update) | async-done | bytes 262160 | tf_op jit(solution)/shard_map/reduce_scatter | solution.py:43
  175.8 1.8 copy.19
  (4 shorter events, 0.0 us)
Async XLA Ops:
  7.2 17.4 %copy-start = (bf16[512,2048]{1,0:T(8,128)(2,1)S(1)}, bf16[512,2048]{1,0:T(8,128)(2,1)}, u32[]{:S(2)}) copy-start(bf16[512,2048]{1,0:T(8,128)(2,1)} %param.13) | copy-start | bytes 6291460
  7.2 92.9 %reduce-scatter.7.cloned.1.call-start = ((), (), s32[]{:S(2)}) async-start(), calls=%async_computation.3 | async-start | bytes 278528
  8.9 4.6 %collective-permute-start = (bf16[30,512]{1,0:T(8,128)(2,1)S(1)}, bf16[30,512]{1,0:T(8,128)(2,1)S(1)}, u32[]{:S(2)}, u32[]{:S(2)}) collective-permute-start(bf16[30,512]{1,0:T(8,128)(2,1)S(1)} %slice.450), channel_id=1, source_target_pairs={{0,2},{2,4},{4,6},{6,8},{8,10},{10,12},{12,14},{14,16},{16,18},{18... | collective-permute-start | bytes 92168 | tf_op jit(solution)/shard_map/ppermute | solution.py:13
  13.6 11.0 %copy-start.4 = (f32[512]{0:T(512)S(1)}, f32[512]{0:T(512)}, u32[]{:S(2)}) copy-start(f32[512]{0:T(512)} %param.10) | copy-start | bytes 6148
  13.6 11.0 %copy-start.5 = (f32[512]{0:T(512)S(1)}, f32[512]{0:T(512)}, u32[]{:S(2)}) copy-start(f32[512]{0:T(512)} %param.11) | copy-start | bytes 6148
  38.3 1.7 copy-start.1
  41.1 134.7 %reduce-scatter.5.cloned.1.call-start = ((), (), s32[]{:S(2)}) async-start(), calls=%async_computation.2 | async-start | bytes 4456448 | tf_op jit(solution)/shard_map/reduce_scatter | solution.py:43
  45.7 1.2 copy-start.2
  47.0 10.3 %copy-start.3 = (bf16[512,512]{1,0:T(8,128)(2,1)S(1)}, bf16[512,512]{1,0:T(8,128)(2,1)}, u32[]{:S(2)}) copy-start(bf16[512,512]{1,0:T(8,128)(2,1)} %param.8) | copy-start | bytes 1572868
  47.0 3.3 %collective-permute-start.1 = (f32[30,512]{1,0:T(8,128)S(1)}, f32[30,512]{1,0:T(8,128)S(1)}, u32[]{:S(2)}, u32[]{:S(2)}) collective-permute-start(f32[30,512]{1,0:T(8,128)S(1)} %slice.482), channel_id=1, source_target_pairs={{2,0},{4,2},{6,4},{8,6},{10,8},{12,10},{14,12},{16,14},{18,16},{20... | collective-permute-start | bytes 184328 | tf_op jit(solution)/shard_map/ppermute | solution.py:13
Sparse Core Ops, SparseCore 0:
  41.2 58.8 reduce-scatter.6
  103.9 71.7 reduce-scatter.4
where the time goes:
time: 185 us; the launch traced here: 184 us
  waiting for transfers between devices  97.3 us (53%)
  blocking collectives  30.4 us (16%)
  other arithmetic  21.5 us (12%)
  between operations  14.2 us (8%)
  matrix products  9.17 us (5%)
  local copies, waits for them, and re-layouts  7.9 us (4%)
  starting transfers between devices  3.9 us (2%)
    reduce_scatter x1, waiting for transfers between devices, on_device(): lax.psum_scatter(lax.dot_general(out_grad, act, (((0,), (0,)), ((), ())),...  53.6 us
    unnamed x3, waiting for transfers between devices  41.8 us
    all_gather x1, blocking collectives, on_device(): summed = lax.all_gather(share, 'sp', axis=1, tiled=True)  20.3 us
    convert_element_type x1, other arithmetic, on_device(): (grad_gated * value * sig_gate * (1.0 - sig_gate)).astype(jnp.bfloat16)  6.99 us
    reduce_sum x2, other arithmetic, on_device(): jnp.sum(conv_output_gradient * padded[k:k + rows], axis=0)  5.89 us
    reduce_sum x1, other arithmetic, on_device(): jnp.sum(conv_output * conv_output, axis=1)  5.75 us
    psum x1, blocking collectives, on_device(): lax.psum((jnp.sum(conv_output, axis=1), jnp.sum(conv_output * conv_output...  5.19 us
    psum x1, blocking collectives, on_device(): lax.psum((jnp.sum(scaled_rows, axis=1), jnp.sum(scaled_rows * centered_st...  4.91 us
  transfers between devices with their start and end apart: 4, of which 3 were waited for; matrix products, arithmetic and copies ran while one was open for 9% of the time, Pallas kernels for 0%

commit v1 on v0

v1 whole, which is shorter than its diff:
```python
import jax
import jax.numpy as jnp
import numpy as np
from jax import lax
from jax.experimental import pallas as pl
from jax.experimental.pallas import tpu as pltpu
from jax.sharding import PartitionSpec as P


def passed_along(shard, axis, by):
    size = lax.axis_size(axis)
    pairs = [(i, i + by) for i in range(size) if 0 <= i + by < size]
    return lax.ppermute(shard, axis, pairs)


def swapped(shard, axis, bit):
    size = lax.axis_size(axis)
    return lax.ppermute(shard, axis, [(i, i ^ (1 << bit)) for i in range(size)])


def bits_of(size):
    bits = size.bit_length() - 1
    return bits if 1 << bits == size else None


def summed_over(shard, axis):
    bits = bits_of(lax.axis_size(axis))
    if bits is None:
        return lax.psum(shard, axis)
    for bit in range(bits):
        shard = shard + swapped(shard, axis, bit)
    return shard


def together(*values):
    return lax.optimization_barrier(values)


def block_products(order, out_grad, act, block, kind):
    def body(order_ref, grad_ref, act_ref, out_ref):
        for n in range(order.shape[0]):
            first = pl.multiple_of(order_ref[n] * block, block)
            out_ref[n] = lax.dot_general(
                grad_ref[:, pl.ds(first, block)],
                act_ref[...],
                (((0,), (0,)), ((), ())),
                preferred_element_type=jnp.float32,
            ).astype(kind)

    vmem = pl.BlockSpec(memory_space=pltpu.VMEM)
    return pl.pallas_call(
        body,
        in_specs=[pl.BlockSpec(memory_space=pltpu.SMEM), vmem, vmem],
        out_specs=vmem,
        out_shape=jax.ShapeDtypeStruct((order.shape[0], block, act.shape[1]), kind),
    )(order, out_grad, act)


def halved(blocks, where, axis, bit):
    kept = lax.index_in_dim(blocks, 0, where, keepdims=False)
    sent = lax.index_in_dim(blocks, 1, where, keepdims=False)
    return kept, swapped(sent.astype(jnp.bfloat16), axis, bit)


def added(pair):
    return pair[0] + pair[1].astype(jnp.float32)


def on_device(
    glu_value, glu_gate, conv_taps, channel_norm_gain, channel_norm_bias, out_proj, out_grad
):
    rows, width = glu_value.shape
    taps = conv_taps.shape[0]
    channels = width * lax.axis_size("tp")
    size = lax.axis_size("sp")
    bits = bits_of(size)
    block = out_grad.shape[1] // size
    by_halves = bits == 4 and block % 128 == 0 and width % 256 == 0

    value = glu_value.astype(jnp.float32)
    sig_gate = jax.nn.sigmoid(glu_gate.astype(jnp.float32))
    gated = (value * sig_gate).astype(jnp.bfloat16)
    before = passed_along(gated[rows - (taps - 1) :], "sp", 1)
    grad_act = lax.dot_general(
        out_grad, out_proj, (((1,), (1,)), ((), ())), preferred_element_type=jnp.float32
    )
    before, grad_act = together(before, grad_act)
    padded = jnp.concatenate([before, gated], axis=0).astype(jnp.float32)
    conv_output = jnp.zeros((rows, width), jnp.float32)
    for k in range(taps):
        conv_output = conv_output + conv_taps[k][None, :] * padded[k : k + rows]
    sums = summed_over(
        jnp.stack([jnp.sum(conv_output, axis=1), jnp.sum(conv_output * conv_output, axis=1)]), "tp"
    )
    channel_mean = (sums[0] / channels)[:, None]
    var = (sums[1] / channels)[:, None] - channel_mean * channel_mean
    inverse_deviation = lax.rsqrt(var + 1e-05)
    centered_standardized = (conv_output - channel_mean) * inverse_deviation
    normalized_rows = (
        centered_standardized * channel_norm_gain[None, :] + channel_norm_bias[None, :]
    )
    sig_norm = jax.nn.sigmoid(normalized_rows)
    act = (normalized_rows * sig_norm).astype(jnp.bfloat16)
    normalized_gradient = grad_act * sig_norm * (1.0 + normalized_rows * (1.0 - sig_norm))
    scaled_rows = normalized_gradient * channel_norm_gain[None, :]
    row_terms = jnp.stack(
        [jnp.sum(scaled_rows, axis=1), jnp.sum(scaled_rows * centered_standardized, axis=1)]
    )
    column_terms = jnp.stack(
        [jnp.sum(normalized_gradient * centered_standardized, axis=0), jnp.sum(normalized_gradient, axis=0)]
    )
    if by_halves:
        relative = np.array(
            [sum(((n >> (bits - 2 - b)) & 1) << (b + 1) for b in range(bits - 1)) for n in range(size // 2)],
            np.int32,
        )
        me = lax.axis_index("sp").astype(jnp.int32)
        act, row_terms = together(act, row_terms)
        sent = block_products(jnp.asarray(relative + 1) ^ me, out_grad, act, block, jnp.bfloat16)
        got = swapped(sent, "sp", 0)
        kept = block_products(jnp.asarray(relative) ^ me, out_grad, act, block, jnp.float32)
        terms = summed_over(row_terms, "tp")
        got, kept, terms = together(got, kept, terms)
        blocks = added((kept, got)).reshape(2, 2, 2, block, width)
        left = halved(blocks[..., : width // 2], 0, "sp", 1)
        right = halved(blocks[..., width // 2 :], 1, "sp", 2)
    else:
        grad_proj = lax.psum_scatter(
            lax.dot_general(
                out_grad, act, (((0,), (0,)), ((), ())), preferred_element_type=jnp.float32
            ),
            "sp",
            scatter_dimension=0,
            tiled=True,
        )
        terms = summed_over(row_terms, "tp")
    conv_output_gradient = inverse_deviation * (
        scaled_rows
        - (terms[0] / channels)[:, None]
        - centered_standardized * (terms[1] / channels)[:, None]
    )
    ahead = passed_along(conv_output_gradient[: taps - 1], "sp", -1)
    taps_local = jnp.stack(
        [jnp.sum(conv_output_gradient * padded[k : k + rows], axis=0) for k in range(taps)], axis=0
    )
    summed = jnp.concatenate([taps_local, column_terms], axis=0)
    if by_halves:
        left, right, summed, ahead, conv_output_gradient = together(
            left, right, summed, ahead, conv_output_gradient
        )
        left = halved(added(left), 0, "sp", 2)
        right = halved(added(right), 0, "sp", 1)
        summed = (summed, swapped(summed, "sp", 0))

    def conv_back(source, count):
        total = jnp.zeros((count, width), jnp.float32)
        for k in range(taps):
            total = total + conv_taps[k][None, :] * source[taps - 1 - k : taps - 1 - k + count]
        return total

    after = jnp.concatenate([conv_output_gradient, ahead], axis=0)
    if by_halves:
        cut = rows // 2
        top = conv_back(after, cut)
        left, right, summed, top, after = together(left, right, summed, top, after)
        both = jnp.concatenate([added(left), added(right)], axis=-1)
        both = halved(both, 0, "sp", 3)
        summed = summed[0] + summed[1]
        summed = (summed, swapped(summed, "sp", 1))
        bottom = conv_back(after[cut:], rows - cut)
        both, summed, bottom = together(both, summed, bottom)
        grad_proj = added(both)
        summed = summed[0] + summed[1]
        for bit in (2, 3):
            summed = summed + swapped(summed, "sp", bit)
        grad_gated = jnp.concatenate([top, bottom], axis=0)
    else:
        summed = summed_over(summed, "sp")
        grad_gated = conv_back(after, rows)
    grad_value = (grad_gated * sig_gate).astype(jnp.bfloat16)
    grad_gate = (grad_gated * value * sig_gate * (1.0 - sig_gate)).astype(jnp.bfloat16)
    return (grad_value, grad_gate, summed[:taps], summed[taps], summed[taps + 1], grad_proj)


def solution(mesh):
    return jax.shard_map(
        on_device,
        mesh=mesh,
        in_specs=(
            P("sp", "tp"),
            P("sp", "tp"),
            P(None, "tp"),
            P("tp"),
            P("tp"),
            P("tp", None),
            P("sp", None),
        ),
        out_specs=(P("sp", "tp"), P("sp", "tp"), P(None, "tp"), P("tp"), P("tp"), P("sp", "tp")),
        check_vma=False,
    )
```

time: 185 us -> 87.6 us (0.47)
  waiting for transfers between devices: 97.3 us -> 15.3 us
  blocking collectives: 30.4 us -> 0 us
  starting transfers between devices: 3.9 us -> 20.6 us
  between operations: 14.2 us -> 2.02 us
  Pallas kernels: 0 us -> 7.26 us
  other arithmetic: 21.5 us -> 27.5 us
  matrix products: 9.17 us -> 3.87 us
  local copies, waits for them, and re-layouts: 7.9 us -> 10.5 us
    reduce_scatter x1 -> x0, waiting for transfers between devices: 53.6 us -> none  [on_device(): lax.psum_scatter(lax.dot_general(out_grad, act, (((0,), (0,)), ((), ())),...]
    unnamed x3 -> x0, waiting for transfers between devices: 41.8 us -> none
    all_gather x1 -> x0, blocking collectives: 20.3 us -> none  [on_device(): summed = lax.all_gather(share, 'sp', axis=1, tiled=True)]
    ppermute x0 -> x12, starting transfers between devices: none -> 16.8 us  [swapped(): return lax.ppermute(shard, axis, [(i, i ^ 1 << bit) for i in range(size)])]
    ppermute x0 -> x12, waiting for transfers between devices: none -> 15.2 us  [swapped(): return lax.ppermute(shard, axis, [(i, i ^ 1 << bit) for i in range(size)])]
    psum x2 -> x0, blocking collectives: 10.1 us -> none  [the longest x1 5.19 us: on_device(): lax.psum((jnp.sum(conv_output, axis=1), jnp.sum(conv_output * conv_output...]
    add x0 -> x14, other arithmetic: none -> 8.32 us  [the longest x6 4.16 us: added(): return pair[0] + pair[1].astype(jnp.float32)]
    pallas_call x0 -> x2, Pallas kernels: none -> 7.26 us  [block_products(): pl.pallas_call(body, in_specs=[pl.BlockSpec(memory_space=pltpu.SMEM), vme...]
  transfers between devices with their start and end apart: 4 -> 14, of which waited for: 3 -> 8; matrix products, arithmetic and copies ran while one was open for 9% -> 18% of each run, Pallas kernels for 0% -> 4%
where the time goes in v1:
time: 87.6 us; the launch traced here: 87 us
  other arithmetic  27.5 us (31%)
  starting transfers between devices  20.6 us (24%)
  waiting for transfers between devices  15.3 us (17%)
  local copies, waits for them, and re-layouts  10.5 us (12%)
  Pallas kernels  7.26 us (8%)
  matrix products  3.87 us (4%)
  between operations  2.02 us (2%)
    ppermute x12, starting transfers between devices, swapped(): return lax.ppermute(shard, axis, [(i, i ^ 1 << bit) for i in range(size)])  16.8 us
    ppermute x12, waiting for transfers between devices, swapped(): return lax.ppermute(shard, axis, [(i, i ^ 1 << bit) for i in range(size)])  15.2 us
    pallas_call x2, Pallas kernels, block_products(): pl.pallas_call(body, in_specs=[pl.BlockSpec(memory_space=pltpu.SMEM), vme...  7.26 us
    reduce_sum x2, other arithmetic, on_device(): jnp.sum(conv_output_gradient * padded[k:k + rows], axis=0)  6.17 us
    reduce_sum x1, other arithmetic, on_device(): jnp.sum(conv_output, axis=1)  5.06 us
    add x6, other arithmetic, added(): return pair[0] + pair[1].astype(jnp.float32)  4.16 us
    add x2, other arithmetic, conv_back(): total + conv_taps[k][None, :] * source[taps - 1 - k:taps - 1 - k + count]  4.09 us
    dot_general x1, matrix products, on_device(): lax.dot_general(out_grad, out_proj, (((1,), (1,)), ((), ())), preferred_e...  3.87 us
  transfers between devices with their start and end apart: 14, of which 8 were waited for; matrix products, arithmetic and copies ran while one was open for 18% of the time, Pallas kernels for 4%

profile of v1, /device:TPU:0, one launch (start us, length us, event | category | flops | bytes accessed | tf_op | source)
XLA Modules:
  0.0 87.0 jit_solution(10359724687178739201)
XLA Ops:
  0.6 0.0 copy-start
  0.6 1.6 %fusion = bf16[512,512]{1,0:T(8,128)(2,1)S(1)} fusion(bf16[512,512]{1,0:T(8,128)(2,1)} %param.9, bf16[512,512]{1,0:T(8,128)(2,1)} %param.10), kind=kLoop, calls=%fused_computation.5 | loop fusion | flops 1835008 | bytes 1572864 | tf_op jit(solution)/shard_map/convert_element_type | solution.py:82
  2.3 0.0 copy-start.6
  2.3 0.8 copy-done.6
  3.1 2.4 %collective-permute-start = (bf16[30,512]{1,0:T(8,128)(2,1)S(1)}, bf16[30,512]{1,0:T(8,128)(2,1)S(1)}, u32[]{:S(2)}, u32[]{:S(2)}) collective-permute-start(bf16[30,512]{1,0:T(8,128)(2,1)S(1)} %slice.708), channel_id=1, source_target_pairs={{0,2},{2,4},{4,6},{6,8},{8,10},{10,12},{12,14},{14,16},{16,18},{18... | collective-permute-start | bytes 92168 | tf_op jit(solution)/shard_map/ppermute | solution.py:13
  5.5 1.2 %fusion.13 = (f32[1,512]{1,0:T(1,128)S(1)}, f32[1,512]{1,0:T(1,128)S(1)}, f32[1,512]{1,0:T(1,128)S(1)}, f32[1,512]{1,0:T(1,128)S(1)}, f32[1,512]{1,0:T(1,128)S(1...) fusion(f32[31,512]{1,0:T(8,128)} %param.11), kind=kLoop, calls=%fused_computation.92 | loop fusion | bytes 77824 | tf_op jit(solution)/shard_map/slice | solution.py:91
  6.9 3.9 %fusion.15 = f32[512,512]{1,0:T(8,128)} fusion(bf16[512,2048]{1,0:T(8,128)(2,1)} %grad_ref.3, bf16[512,2048]{1,0:T(8,128)(2,1)S(1)} %copy-done), kind=kOutput, calls=%fused_computation.94 | convolution fusion | flops 1073741824 | bytes 5242880 | tf_op jit(solution)/shard_map/dot_general | solution.py:84
  10.7 1.0 %fusion.14 = (f32[1,512]{1,0:T(1,128)S(1)}, f32[1,512]{1,0:T(1,128)S(1)}, f32[1,512]{1,0:T(1,128)S(1)}, f32[1,512]{1,0:T(1,128)S(1)}, f32[1,512]{1,0:T(1,128)S(1...) fusion(f32[31,512]{1,0:T(8,128)} %param.11), kind=kLoop, calls=%fused_computation.93 | loop fusion | bytes 49152 | tf_op jit(solution)/shard_map/slice | solution.py:91
  11.9 0.0 collective-permute-done
  11.9 1.2 %maximum_convert_fusion = f32[542,512]{1,0:T(8,128)S(1)} fusion(bf16[512,512]{1,0:T(8,128)(2,1)} %copy-done.6, bf16[30,512]{1,0:T(8,128)(2,1)S(1)} %collective-permute-done), kind=kLoop, calls=%fused_computation.53 | loop fusion | flops 1110016 | bytes 1665024 | tf_op jit(solution)/shard_map/convert_element_type | solution.py:88
  13.3 0.0 copy-start.75
  13.3 0.0 copy-start.72
  13.3 0.0 copy-start.73
  13.3 5.1 %fusion.11 = (f32[512]{0:T(512)S(1)}, f32[512]{0:T(512)S(1)}, f32[512,512]{1,0:T(8,128)S(1)}) fusion(f32[542,512]{1,0:T(8,128)S(1)} %maximum_convert_fusion, f32[512]{0:T(512)S(1)} %bitcast.191, f32[512]{0:T(512)S(1)} %bitcast.194, f32[512]{0:T(512)S(1)} %bitcast.107, f32[512]{0:T(512)S(1)} %bitcast.110, f32[512]{0:T(512)S(1)} %bitcast.113, ...), kind=kLoop, calls=%fused_computation.90 | loop fusion | flops 16776192 | bytes 33622016 | tf_op jit(solution)/shard_map/reduce_sum | solution.py:93
  18.5 2.4 %collective-permute-start.1 = (f32[2,512]{1,0:T(2,128)S(1)}, f32[2,512]{1,0:T(2,128)S(1)}, u32[]{:S(2)}, u32[]{:S(2)}) collective-permute-start(f32[2,512]{1,0:T(2,128)S(1)} %pad_maximum_fusion.2), channel_id=1, source_target_pairs={{0,1},{1,0},{2,3},{3,2},{4,5},{5,4},{6,7},{7,6},{8,9},{9,8},{10,11... | collective-permute-start | bytes 12296 | tf_op jit(solution)/shard_map/ppermute | solution.py:18
  20.9 0.0 copy-done.75
  20.9 0.5 broadcast_xor_fusion.1.order_ref
  21.4 1.1 %collective-permute-done.1 = f32[2,512]{1,0:T(2,128)S(1)} collective-permute-done((f32[2,512]{1,0:T(2,128)S(1)}, f32[2,512]{1,0:T(2,128)S(1)}, u32[]{:S(2)}, u32[]{:S(2)}) %collective-permute-start.1) | collective-permute-done | bytes 4128 | tf_op jit(solution)/shard_map/ppermute | solution.py:18
  22.6 2.5 %multiply_reduce_fusion = (f32[512]{0:T(512)}, f32[512]{0:T(512)S(1)}, f32[512]{0:T(512)S(1)}, f32[512]{0:T(512)}, f32[512,512]{1,0:T(8,128)}, /*index=5*/bf16[512,512]{1,0:T(8,128)(2,1)}) fusion(f32[512,512]{1,0:T(8,128)S(1)} %get-tuple-element.99, f32[512]{0:T(512)S(1)} %add_rsqrt_fusion, f32[512]{0:T(512)S(1)} %bitcast.102, f32[512]{0:T(512)S(1)} %copy-done.72, ...), kind=kLoop, calls=%fused_computation.10 | loop fusion | flops 5502976 | bytes 3686400 | tf_op jit(solution)/shard_map/reduce_sum | solution.py:110
  25.1 3.5 %shard_map.136 = bf16[8,128,512]{2,1,0:T(8,128)(2,1)} custom-call(s32[8]{0:T(128)} %broadcast_xor_fusion.1.order_ref, bf16[512,2048]{1,0:T(8,128)(2,1)} %grad_ref.3, bf16[512,512]{1,0:T(8,128)(2,1)} %get-tuple-element.35.act_ref), custom_call_target="tpu_custom_call" | custom-call | tf_op jit(solution)/shard_map/pallas_call | solution.py:51
  28.6 1.2 %collective-permute-start.2 = (bf16[8,128,512]{2,1,0:T(8,128)(2,1)}, bf16[8,128,512]{2,1,0:T(8,128)(2,1)}, u32[]{:S(2)}, u32[]{:S(2)}) collective-permute-start(bf16[8,128,512]{2,1,0:T(8,128)(2,1)} %shard_map.136), channel_id=1, source_target_pairs={{0,2},{2,0},{4,6},{6,4},{8,10},{10,8},{12,14},{14,12},{16,18},{18,... | collective-permute-start | bytes 3145736 | tf_op jit(solution)/shard_map/ppermute | solution.py:18
  29.7 1.5 %collective-permute-start.3 = (f32[2,512]{1,0:T(2,128)S(1)}, f32[2,512]{1,0:T(2,128)S(1)}, u32[]{:S(2)}, u32[]{:S(2)}) collective-permute-start(f32[2,512]{1,0:T(2,128)S(1)} %pad_maximum_fusion.3), channel_id=1, source_target_pairs={{0,1},{1,0},{2,3},{3,2},{4,5},{5,4},{6,7},{7,6},{8,9},{9,8},{10,11... | collective-permute-start | bytes 12296 | tf_op jit(solution)/shard_map/ppermute | solution.py:18
  31.2 0.5 broadcast_xor_fusion.order_ref
  31.7 3.8 %shard_map.137 = f32[8,128,512]{2,1,0:T(8,128)} custom-call(s32[8]{0:T(128)} %broadcast_xor_fusion.order_ref, bf16[512,2048]{1,0:T(8,128)(2,1)} %grad_ref.3, bf16[512,512]{1,0:T(8,128)(2,1)} %get-tuple-element.35.act_ref), custom_call_target="tpu_custom_call" | custom-call | tf_op jit(solution)/shard_map/pallas_call | solution.py:51
  35.5 0.0 collective-permute-done.3
  35.6 0.0 collective-permute-done.2
  35.6 2.3 %convert_add_fusion = f32[8,128,512]{2,1,0:T(8,128)S(1)} fusion(f32[8,128,512]{2,1,0:T(8,128)} %shard_map.137, bf16[8,128,512]{2,1,0:T(8,128)(2,1)} %collective-permute-done.2), kind=kLoop, calls=%fused_computation.1 | loop fusion | flops 1048576 | bytes 5242880 | tf_op jit(solution)/shard_map/add | solution.py:66
  37.9 0.7 slice_bitcast_fusion.5
  38.7 0.7 slice_bitcast_fusion.4
  39.4 3.8 %multiply_reduce_fusion.1 = (f32[512]{0:T(512)}, f32[512]{0:T(512)}, f32[512]{0:T(512)}, f32[512]{0:T(512)}, f32[512]{0:T(512)}, /*index=5*/f32[512]{0:T(512)}, ...) fusion(f32[542,512]{1,0:T(8,128)S(1)} %maximum_convert_fusion, ...), kind=kLoop, calls=%fused_computation.11 | loop fusion | flops 11262976 | bytes 22067200 | tf_op jit(solution)/shard_map/reduce_sum | solution.py:144
  43.3 2.3 %multiply_reduce_fusion.19 = (f32[512]{0:T(512)}, f32[512]{0:T(512)}, f32[512]{0:T(512)}, f32[512]{0:T(512)}, f32[512]{0:T(512)}, /*index=5*/f32[512]{0:T(512)},...) fusion(f32[512,512]{1,0:T(8,128)S(1)} %get-tuple-element.45, ...), kind=kLoop, calls=%fused_computation.29 | loop fusion | flops 6809088 | bytes 14706688 | tf_op jit(solution)/shard_map/reduce_sum | solution.py:144
  45.6 1.5 %collective-permute-start.4 = (bf16[2,2,128,256]{3,2,1,0:T(8,128)(2,1)}, bf16[2,2,128,256]{3,2,1,0:T(8,128)(2,1)S(1)}, u32[]{:S(2)}, u32[]{:S(2)}) collective-permute-start(bf16[2,2,128,256]{3,2,1,0:T(8,128)(2,1)} %slice_bitcast_fusion.5), channel_id=1, source_target_pairs={{0,4},{2,6},{4,0},{6,2},{8,12},{10,14},{12,8},{14,10},{16,20},{18,... | collective-permute-start | bytes 786440 | tf_op jit(solution)/shard_map/ppermute | solution.py:18
  47.1 1.6 %collective-permute-start.5 = (bf16[2,2,128,256]{3,2,1,0:T(8,128)(2,1)}, bf16[2,2,128,256]{3,2,1,0:T(8,128)(2,1)}, u32[]{:S(2)}, u32[]{:S(2)}) collective-permute-start(bf16[2,2,128,256]{3,2,1,0:T(8,128)(2,1)} %slice_bitcast_fusion.4), channel_id=1, source_target_pairs={{0,8},{2,10},{4,12},{6,14},{8,0},{10,2},{12,4},{14,6},{16,24},{18,... | collective-permute-start | bytes 786440 | tf_op jit(solution)/shard_map/ppermute | solution.py:18
  48.7 0.6 slice.746
  49.4 1.5 %collective-permute-start.6 = (f32[30,512]{1,0:T(8,128)}, f32[30,512]{1,0:T(8,128)S(1)}, u32[]{:S(2)}, u32[]{:S(2)}) collective-permute-start(f32[30,512]{1,0:T(8,128)} %slice.746), channel_id=1, source_target_pairs={{2,0},{4,2},{6,4},{8,6},{10,8},{12,10},{14,12},{16,14},{18,16},{20... | collective-permute-start | bytes 184328 | tf_op jit(solution)/shard_map/ppermute | solution.py:13
  50.9 3.7 %concatenate.16 = f32[33,512]{1,0:T(8,128)S(1)} concatenate(f32[1,512]{1,0:T(1,128)} %bitcast.235, f32[1,512]{1,0:T(1,128)} %bitcast.234, f32[1,512]{1,0:T(1,128)} %bitcast.233, f32[1,512]{1,0:T(1,128)} %bitcast.232, f32[1,512]{1,0:T(1,128)} %bitcast.231, f32[1,512]{1,0:T(1,128)} %bitcast.230, f32[1,512]{1,0:T(1,128)} %bitcast.229, f32[1,512]{1,0:T(1,128)} %bitcast.228, ...), dimensions={0} | concatenate | bytes 135168 | tf_op jit(solution)/shard_map/concatenate | solution.py:146
  54.8 0.0 collective-permute-done.6
  54.9 0.0 collective-permute-done.4
  54.9 0.3 collective-permute-done.5
  55.2 0.1 convert_add_fusion.2
  55.2 1.0 %convert_add_fusion.1 = f32[2,2,128,256]{3,2,1,0:T(8,128)S(1)} fusion(f32[2,2,128,256]{3,2,1,0:T(8,128)S(1)} %slice_bitcast_fusion, bf16[2,2,128,256]{3,2,1,0:T(8,128)(2,1)} %collective-permute-done.5), kind=kLoop, calls=%fused_computation.60 | loop fusion | flops 262144 | bytes 1310720 | tf_op jit(solution)/shard_map/add | solution.py:66
  56.6 2.1 %multiply_add_fusion.3 = f32[256,512]{1,0:T(8,128)S(1)} fusion(f32[512,512]{1,0:T(8,128)S(1)} %copy-done.2, f32[512]{0:T(512)S(1)} %bitcast.192, f32[512]{0:T(512)S(1)} %bitcast.195, f32[512]{0:T(512)S(1)} %bitcast.108, f32[512]{0:T(512)S(1)} %bitcast.111, f32[512]{0:T(512)S(1)} %bitcast.114, f32[512]{0:T(512)S(1)} %bitcast.117, f32[512]{0:T(512)S(1)} %bitcast.120, ...), kind=kLoop, calls=%fused_computation.59 | loop fusion | flops 7995392 | bytes 16840704 | tf_op jit(solution)/shard_map/add | solution.py:158
  58.7 1.6 %collective-permute-start.7 = (bf16[2,128,256]{2,1,0:T(8,128)(2,1)S(1)}, bf16[2,128,256]{2,1,0:T(8,128)(2,1)S(1)}, u32[]{:S(2)}, u32[]{:S(2)}) collective-permute-start(bf16[2,128,256]{2,1,0:T(8,128)(2,1)S(1)} %fusion.7), channel_id=1, source_target_pairs={{0,8},{2,10},{4,12},{6,14},{8,0},{10,2},{12,4},{14,6},{16,24},{18,... | collective-permute-start | bytes 393224 | tf_op jit(solution)/shard_map/ppermute | solution.py:18
  60.4 0.5 collective-permute-start.8
  60.9 0.0 collective-permute-start.9
  60.9 0.1 pad_maximum_fusion
  61.0 1.2 %collective-permute-done.9 = f32[33,512]{1,0:T(8,128)S(1)} collective-permute-done((f32[33,512]{1,0:T(8,128)S(1)}, f32[33,512]{1,0:T(8,128)S(1)}, u32[]{:S(2)}, u32[]{:S(2)}) %collective-permute-start.9) | collective-permute-done | bytes 67616 | tf_op jit(solution)/shard_map/ppermute | solution.py:18
  62.1 2.9 %collective-permute-done.7 = bf16[2,128,256]{2,1,0:T(8,128)(2,1)S(1)} collective-permute-done((bf16[2,128,256]{2,1,0:T(8,128)(2,1)S(1)}, bf16[2,128,256]{2,1,0:T(8,128)(2,1)S(1)}, u32[]{:S(2)}, u32[]{:S(2)}) %collective-permute-start.7) | collective-permute-done | bytes 131104 | tf_op jit(solution)/shard_map/ppermute | solution.py:18
  65.1 0.3 collective-permute-done.8
  65.3 1.2 %collective-permute-start.11 = (f32[33,512]{1,0:T(8,128)S(1)}, f32[33,512]{1,0:T(8,128)S(1)}, u32[]{:S(2)}, u32[]{:S(2)}) collective-permute-start(f32[33,512]{1,0:T(8,128)S(1)} %add.408), channel_id=1, source_target_pairs={{0,4},{2,6},{4,0},{6,2},{8,12},{10,14},{12,8},{14,10},{16,20},{18,... | collective-permute-start | bytes 202760 | tf_op jit(solution)/shard_map/ppermute | solution.py:18
  66.6 2.4 %collective-permute-start.10 = (bf16[128,512]{1,0:T(8,128)(2,1)S(1)}, bf16[128,512]{1,0:T(8,128)(2,1)S(1)}, u32[]{:S(2)}, u32[]{:S(2)}) collective-permute-start(bf16[128,512]{1,0:T(8,128)(2,1)S(1)} %fusion.9), channel_id=1, source_target_pairs={{0,16},{2,18},{4,20},{6,22},{8,24},{10,26},{12,28},{14,30},{16,0},... | collective-permute-start | bytes 393224 | tf_op jit(solution)/shard_map/ppermute | solution.py:18
  69.0 2.0 %multiply_add_fusion.2 = f32[256,512]{1,0:T(8,128)S(1)} fusion(f32[542,512]{1,0:T(8,128)S(1)} %pad_maximum_fusion, f32[512]{0:T(512)S(1)} %bitcast.193, f32[512]{0:T(512)S(1)} %bitcast.196, f32[512]{0:T(512)S(1)} %bitcast.109, f32[512]{0:T(512)S(1)} %bitcast.112, f32[512]{0:T(512)S(1)} %bitcast.115, f32[512]{0:T(512)S(1)} %bitcast.118, f32[512]{0:T(512)S(1)} %bitcast.121, ...), kind=kLoop, calls=%fused_computation.58 | loop fusion | flops 7995392 | bytes 16840704 | tf_op jit(solution)/shard_map/add | solution.py:158
  71.0 0.0 copy-start.7
  71.0 0.0 copy-start.8
  71.1 0.0 collective-permute-done.11
  71.1 3.8 %collective-permute-done.10 = bf16[128,512]{1,0:T(8,128)(2,1)S(1)} collective-permute-done((bf16[128,512]{1,0:T(8,128)(2,1)S(1)}, bf16[128,512]{1,0:T(8,128)(2,1)S(1)}, u32[]{:S(2)}, u32[]{:S(2)}) %collective-permute-start.10) | collective-permute-done | bytes 131104 | tf_op jit(solution)/shard_map/ppermute | solution.py:18
  75.0 0.7 collective-permute-start.12
  75.7 1.4 %fusion.3 = (bf16[512,512]{1,0:T(8,128)(2,1)}, bf16[512,512]{1,0:T(8,128)(2,1)}) fusion(f32[512,512]{1,0:T(8,128)S(1)} %constant_dynamic-update-slice_fusion, bf16[512,512]{1,0:T(8,128)(2,1)S(1)} %copy-done.7, bf16[512,512]{1,0:T(8,128)(2,1)S(1)} %copy-done.8), kind=kLoop, calls=%fused_computation.8 | loop fusion | flops 3145728 | bytes 3145728 | tf_op jit(solution)/shard_map/convert_element_type | solution.py:181
  77.1 2.3 %collective-permute-done.12 = f32[33,512]{1,0:T(8,128)S(1)} collective-permute-done((f32[33,512]{1,0:T(8,128)S(1)}, f32[33,512]{1,0:T(8,128)S(1)}, u32[]{:S(2)}, u32[]{:S(2)}) %collective-permute-start.12) | collective-permute-done | bytes 67616 | tf_op jit(solution)/shard_map/ppermute | solution.py:18
  79.5 2.2 %collective-permute-start.13 = (f32[33,512]{1,0:T(8,128)S(1)}, f32[33,512]{1,0:T(8,128)S(1)}, u32[]{:S(2)}, u32[]{:S(2)}) collective-permute-start(f32[33,512]{1,0:T(8,128)S(1)} %add.440), channel_id=1, source_target_pairs={{0,16},{2,18},{4,20},{6,22},{8,24},{10,26},{12,28},{14,30},{16,0},... | collective-permute-start | bytes 202760 | tf_op jit(solution)/shard_map/ppermute | solution.py:18
  81.7 0.7 convert_add_fusion.3
  82.5 3.3 %collective-permute-done.13 = f32[33,512]{1,0:T(8,128)S(1)} collective-permute-done((f32[33,512]{1,0:T(8,128)S(1)}, f32[33,512]{1,0:T(8,128)S(1)}, u32[]{:S(2)}, u32[]{:S(2)}) %collective-permute-start.13) | collective-permute-done | bytes 67616 | tf_op jit(solution)/shard_map/ppermute | solution.py:18
  85.8 0.6 slice.753
  86.4 0.6 fusion.12
  (166 shorter events, 0.7 us)
Async XLA Ops:
  0.6 6.0 %copy-start = (bf16[512,2048]{1,0:T(8,128)(2,1)S(1)}, bf16[512,2048]{1,0:T(8,128)(2,1)}, u32[]{:S(2)}) copy-start(bf16[512,2048]{1,0:T(8,128)(2,1)} %param.14) | copy-start | bytes 6291460
  3.1 8.8 %collective-permute-start = (bf16[30,512]{1,0:T(8,128)(2,1)S(1)}, bf16[30,512]{1,0:T(8,128)(2,1)S(1)}, u32[]{:S(2)}, u32[]{:S(2)}) collective-permute-start(bf16[30,512]{1,0:T(8,128)(2,1)S(1)} %slice.708), channel_id=1, source_target_pairs={{0,2},{2,4},{4,6},{6,8},{8,10},{10,12},{12,14},{14,16},{16,18},{18... | collective-permute-start | bytes 92168 | tf_op jit(solution)/shard_map/ppermute | solution.py:13
  6.7 6.4 %copy-start.10 = (f32[1,512]{1,0:T(1,128)}, f32[1,512]{1,0:T(1,128)S(1)}, u32[]{:S(2)}) copy-start(f32[1,512]{1,0:T(1,128)S(1)} %get-tuple-element.105) | copy-start | bytes 6148
  6.7 6.4 %copy-start.12 = (f32[1,512]{1,0:T(1,128)}, f32[1,512]{1,0:T(1,128)S(1)}, u32[]{:S(2)}) copy-start(f32[1,512]{1,0:T(1,128)S(1)} %get-tuple-element.106) | copy-start | bytes 6148
  6.7 6.4 %copy-start.14 = (f32[1,512]{1,0:T(1,128)}, f32[1,512]{1,0:T(1,128)S(1)}, u32[]{:S(2)}) copy-start(f32[1,512]{1,0:T(1,128)S(1)} %get-tuple-element.107) | copy-start | bytes 6148
  6.7 6.4 %copy-start.16 = (f32[1,512]{1,0:T(1,128)}, f32[1,512]{1,0:T(1,128)S(1)}, u32[]{:S(2)}) copy-start(f32[1,512]{1,0:T(1,128)S(1)} %get-tuple-element.108) | copy-start | bytes 6148
  6.7 6.4 %copy-start.18 = (f32[1,512]{1,0:T(1,128)}, f32[1,512]{1,0:T(1,128)S(1)}, u32[]{:S(2)}) copy-start(f32[1,512]{1,0:T(1,128)S(1)} %get-tuple-element.109) | copy-start | bytes 6148
  6.7 6.4 %copy-start.20 = (f32[1,512]{1,0:T(1,128)}, f32[1,512]{1,0:T(1,128)S(1)}, u32[]{:S(2)}) copy-start(f32[1,512]{1,0:T(1,128)S(1)} %get-tuple-element.110) | copy-start | bytes 6148
  6.7 6.4 %copy-start.22 = (f32[1,512]{1,0:T(1,128)}, f32[1,512]{1,0:T(1,128)S(1)}, u32[]{:S(2)}) copy-start(f32[1,512]{1,0:T(1,128)S(1)} %get-tuple-element.111) | copy-start | bytes 6148
  6.8 6.4 %copy-start.24 = (f32[1,512]{1,0:T(1,128)}, f32[1,512]{1,0:T(1,128)S(1)}, u32[]{:S(2)}) copy-start(f32[1,512]{1,0:T(1,128)S(1)} %get-tuple-element.112) | copy-start | bytes 6148
  6.8 6.4 %copy-start.26 = (f32[1,512]{1,0:T(1,128)}, f32[1,512]{1,0:T(1,128)S(1)}, u32[]{:S(2)}) copy-start(f32[1,512]{1,0:T(1,128)S(1)} %get-tuple-element.113) | copy-start | bytes 6148
  6.8 6.4 %copy-start.28 = (f32[1,512]{1,0:T(1,128)}, f32[1,512]{1,0:T(1,128)S(1)}, u32[]{:S(2)}) copy-start(f32[1,512]{1,0:T(1,128)S(1)} %get-tuple-element.114) | copy-start | bytes 6148
  6.8 6.4 %copy-start.30 = (f32[1,512]{1,0:T(1,128)}, f32[1,512]{1,0:T(1,128)S(1)}, u32[]{:S(2)}) copy-start(f32[1,512]{1,0:T(1,128)S(1)} %get-tuple-element.115) | copy-start | bytes 6148
  6.8 6.4 %copy-start.32 = (f32[1,512]{1,0:T(1,128)}, f32[1,512]{1,0:T(1,128)S(1)}, u32[]{:S(2)}) copy-start(f32[1,512]{1,0:T(1,128)S(1)} %get-tuple-element.116) | copy-start | bytes 6148
  6.8 6.4 %copy-start.34 = (f32[1,512]{1,0:T(1,128)}, f32[1,512]{1,0:T(1,128)S(1)}, u32[]{:S(2)}) copy-start(f32[1,512]{1,0:T(1,128)S(1)} %get-tuple-element.117) | copy-start | bytes 6148
  6.8 6.4 %copy-start.36 = (f32[1,512]{1,0:T(1,128)}, f32[1,512]{1,0:T(1,128)S(1)}, u32[]{:S(2)}) copy-start(f32[1,512]{1,0:T(1,128)S(1)} %get-tuple-element.118) | copy-start | bytes 6148
  6.8 6.4 %copy-start.38 = (f32[1,512]{1,0:T(1,128)}, f32[1,512]{1,0:T(1,128)S(1)}, u32[]{:S(2)}) copy-start(f32[1,512]{1,0:T(1,128)S(1)} %get-tuple-element.119) | copy-start | bytes 6148
  6.8 6.4 %copy-start.40 = (f32[1,512]{1,0:T(1,128)}, f32[1,512]{1,0:T(1,128)S(1)}, u32[]{:S(2)}) copy-start(f32[1,512]{1,0:T(1,128)S(1)} %get-tuple-element.120) | copy-start | bytes 6148
  6.8 6.4 %copy-start.42 = (f32[1,512]{1,0:T(1,128)}, f32[1,512]{1,0:T(1,128)S(1)}, u32[]{:S(2)}) copy-start(f32[1,512]{1,0:T(1,128)S(1)} %get-tuple-element.121) | copy-start | bytes 6148
  6.9 6.4 %copy-start.44 = (f32[1,512]{1,0:T(1,128)}, f32[1,512]{1,0:T(1,128)S(1)}, u32[]{:S(2)}) copy-start(f32[1,512]{1,0:T(1,128)S(1)} %get-tuple-element.122) | copy-start | bytes 6148
  6.9 6.4 %copy-start.46 = (f32[1,512]{1,0:T(1,128)}, f32[1,512]{1,0:T(1,128)S(1)}, u32[]{:S(2)}) copy-start(f32[1,512]{1,0:T(1,128)S(1)} %get-tuple-element.123) | copy-start | bytes 6148
  11.8 6.6 %copy-start.48 = (f32[1,512]{1,0:T(1,128)}, f32[1,512]{1,0:T(1,128)S(1)}, u32[]{:S(2)}) copy-start(f32[1,512]{1,0:T(1,128)S(1)} %get-tuple-element.124) | copy-start | bytes 6148
  11.8 6.6 %copy-start.50 = (f32[1,512]{1,0:T(1,128)}, f32[1,512]{1,0:T(1,128)S(1)}, u32[]{:S(2)}) copy-start(f32[1,512]{1,0:T(1,128)S(1)} %get-tuple-element.125) | copy-start | bytes 6148
  11.8 6.6 %copy-start.52 = (f32[1,512]{1,0:T(1,128)}, f32[1,512]{1,0:T(1,128)S(1)}, u32[]{:S(2)}) copy-start(f32[1,512]{1,0:T(1,128)S(1)} %get-tuple-element.126) | copy-start | bytes 6148
  11.8 6.6 %copy-start.54 = (f32[1,512]{1,0:T(1,128)}, f32[1,512]{1,0:T(1,128)S(1)}, u32[]{:S(2)}) copy-start(f32[1,512]{1,0:T(1,128)S(1)} %get-tuple-element.127) | copy-start | bytes 6148
  11.8 6.6 %copy-start.56 = (f32[1,512]{1,0:T(1,128)}, f32[1,512]{1,0:T(1,128)S(1)}, u32[]{:S(2)}) copy-start(f32[1,512]{1,0:T(1,128)S(1)} %get-tuple-element.128) | copy-start | bytes 6148
  11.8 6.6 %copy-start.58 = (f32[1,512]{1,0:T(1,128)}, f32[1,512]{1,0:T(1,128)S(1)}, u32[]{:S(2)}) copy-start(f32[1,512]{1,0:T(1,128)S(1)} %get-tuple-element.129) | copy-start | bytes 6148
  11.8 6.6 %copy-start.60 = (f32[1,512]{1,0:T(1,128)}, f32[1,512]{1,0:T(1,128)S(1)}, u32[]{:S(2)}) copy-start(f32[1,512]{1,0:T(1,128)S(1)} %get-tuple-element.130) | copy-start | bytes 6148
  11.8 6.6 %copy-start.62 = (f32[1,512]{1,0:T(1,128)}, f32[1,512]{1,0:T(1,128)S(1)}, u32[]{:S(2)}) copy-start(f32[1,512]{1,0:T(1,128)S(1)} %get-tuple-element.131) | copy-start | bytes 6148
  11.8 6.6 %copy-start.64 = (f32[1,512]{1,0:T(1,128)}, f32[1,512]{1,0:T(1,128)S(1)}, u32[]{:S(2)}) copy-start(f32[1,512]{1,0:T(1,128)S(1)} %get-tuple-element.132) | copy-start | bytes 6148
  11.8 6.6 %copy-start.66 = (f32[1,512]{1,0:T(1,128)}, f32[1,512]{1,0:T(1,128)S(1)}, u32[]{:S(2)}) copy-start(f32[1,512]{1,0:T(1,128)S(1)} %get-tuple-element.133) | copy-start | bytes 6148
  11.9 6.6 %copy-start.68 = (f32[1,512]{1,0:T(1,128)}, f32[1,512]{1,0:T(1,128)S(1)}, u32[]{:S(2)}) copy-start(f32[1,512]{1,0:T(1,128)S(1)} %get-tuple-element.134) | copy-start | bytes 6148
  11.9 6.6 %copy-start.70 = (f32[1,512]{1,0:T(1,128)}, f32[1,512]{1,0:T(1,128)S(1)}, u32[]{:S(2)}) copy-start(f32[1,512]{1,0:T(1,128)S(1)} %get-tuple-element.135) | copy-start | bytes 6148
  13.3 7.6 %copy-start.75 = (s32[8]{0:T(128)S(1)}, s32[8]{0:T(128)}, u32[]{:S(2)}) copy-start(s32[8]{0:T(128)} %constant.22.clone) | copy-start | bytes 100
  13.3 9.3 %copy-start.9 = (f32[512,512]{1,0:T(8,128)S(1)}, f32[512,512]{1,0:T(8,128)}, u32[]{:S(2)}) copy-start(f32[512,512]{1,0:T(8,128)} %fusion.15) | copy-start | bytes 3145732
  13.3 9.3 %copy-start.72 = (f32[512]{0:T(512)S(1)}, f32[512]{0:T(512)}, u32[]{:S(2)}) copy-start(f32[512]{0:T(512)} %param.12) | copy-start | bytes 6148
  13.3 9.3 %copy-start.73 = (f32[512]{0:T(512)S(1)}, f32[512]{0:T(512)}, u32[]{:S(2)}) copy-start(f32[512]{0:T(512)} %param.13) | copy-start | bytes 6148
  18.5 4.0 %copy-start.3 = (f32[512,512]{1,0:T(8,128)}, f32[512,512]{1,0:T(8,128)S(1)}, u32[]{:S(2)}) copy-start(f32[512,512]{1,0:T(8,128)S(1)} %get-tuple-element.99) | copy-start | bytes 3145732
  18.5 4.0 %collective-permute-start.1 = (f32[2,512]{1,0:T(2,128)S(1)}, f32[2,512]{1,0:T(2,128)S(1)}, u32[]{:S(2)}, u32[]{:S(2)}) collective-permute-start(f32[2,512]{1,0:T(2,128)S(1)} %pad_maximum_fusion.2), channel_id=1, source_target_pairs={{0,1},{1,0},{2,3},{3,2},{4,5},{5,4},{6,7},{7,6},{8,9},{9,8},{10,11... | collective-permute-start | bytes 12296 | tf_op jit(solution)/shard_map/ppermute | solution.py:18
  25.1 6.1 %copy-start.74 = (s32[8]{0:T(128)S(1)}, s32[8]{0:T(128)}, u32[]{:S(2)}) copy-start(s32[8]{0:T(128)} %constant.23.clone) | copy-start | bytes 100
  28.6 7.0 %collective-permute-start.2 = (bf16[8,128,512]{2,1,0:T(8,128)(2,1)}, bf16[8,128,512]{2,1,0:T(8,128)(2,1)}, u32[]{:S(2)}, u32[]{:S(2)}) collective-permute-start(bf16[8,128,512]{2,1,0:T(8,128)(2,1)} %shard_map.136), channel_id=1, source_target_pairs={{0,2},{2,0},{4,6},{6,4},{8,10},{10,8},{12,14},{14,12},{16,18},{18,... | collective-permute-start | bytes 3145736 | tf_op jit(solution)/shard_map/ppermute | solution.py:18
  29.7 5.8 %collective-permute-start.3 = (f32[2,512]{1,0:T(2,128)S(1)}, f32[2,512]{1,0:T(2,128)S(1)}, u32[]{:S(2)}, u32[]{:S(2)}) collective-permute-start(f32[2,512]{1,0:T(2,128)S(1)} %pad_maximum_fusion.3), channel_id=1, source_target_pairs={{0,1},{1,0},{2,3},{3,2},{4,5},{5,4},{6,7},{7,6},{8,9},{9,8},{10,11... | collective-permute-start | bytes 12296 | tf_op jit(solution)/shard_map/ppermute | solution.py:18
  35.6 3.8 %copy-start.4 = (f32[512,512]{1,0:T(8,128)S(1)}, f32[512,512]{1,0:T(8,128)}, u32[]{:S(2)}) copy-start(f32[512,512]{1,0:T(8,128)} %copy-done.3) | copy-start | bytes 3145732
  35.6 3.8 %copy-start.5 = (f32[512,512]{1,0:T(8,128)S(1)}, f32[512,512]{1,0:T(8,128)}, u32[]{:S(2)}) copy-start(f32[512,512]{1,0:T(8,128)} %get-tuple-element.98) | copy-start | bytes 3145732
  43.3 5.4 %copy-start.1 = (f32[512,512]{1,0:T(8,128)}, f32[512,512]{1,0:T(8,128)S(1)}, u32[]{:S(2)}) copy-start(f32[512,512]{1,0:T(8,128)S(1)} %get-tuple-element.45) | copy-start | bytes 3145732
  45.6 9.3 %collective-permute-start.4 = (bf16[2,2,128,256]{3,2,1,0:T(8,128)(2,1)}, bf16[2,2,128,256]{3,2,1,0:T(8,128)(2,1)S(1)}, u32[]{:S(2)}, u32[]{:S(2)}) collective-permute-start(bf16[2,2,128,256]{3,2,1,0:T(8,128)(2,1)} %slice_bitcast_fusion.5), channel_id=1, source_target_pairs={{0,4},{2,6},{4,0},{6,2},{8,12},{10,14},{12,8},{14,10},{16,20},{18,... | collective-permute-start | bytes 786440 | tf_op jit(solution)/shard_map/ppermute | solution.py:18
  47.1 8.1 %collective-permute-start.5 = (bf16[2,2,128,256]{3,2,1,0:T(8,128)(2,1)}, bf16[2,2,128,256]{3,2,1,0:T(8,128)(2,1)}, u32[]{:S(2)}, u32[]{:S(2)}) collective-permute-start(bf16[2,2,128,256]{3,2,1,0:T(8,128)(2,1)} %slice_bitcast_fusion.4), channel_id=1, source_target_pairs={{0,8},{2,10},{4,12},{6,14},{8,0},{10,2},{12,4},{14,6},{16,24},{18,... | collective-permute-start | bytes 786440 | tf_op jit(solution)/shard_map/ppermute | solution.py:18
  49.4 5.5 %collective-permute-start.6 = (f32[30,512]{1,0:T(8,128)}, f32[30,512]{1,0:T(8,128)S(1)}, u32[]{:S(2)}, u32[]{:S(2)}) collective-permute-start(f32[30,512]{1,0:T(8,128)} %slice.746), channel_id=1, source_target_pairs={{2,0},{4,2},{6,4},{8,6},{10,8},{12,10},{14,12},{16,14},{18,16},{20... | collective-permute-start | bytes 184328 | tf_op jit(solution)/shard_map/ppermute | solution.py:13
  54.6 1.8 %copy-start.15 = (f32[1,512]{1,0:T(1,128)S(1)}, f32[1,512]{1,0:T(1,128)}, u32[]{:S(2)}) copy-start(f32[1,512]{1,0:T(1,128)} %copy-done.14) | copy-start | bytes 6148
  54.6 1.8 %copy-start.17 = (f32[1,512]{1,0:T(1,128)S(1)}, f32[1,512]{1,0:T(1,128)}, u32[]{:S(2)}) copy-start(f32[1,512]{1,0:T(1,128)} %copy-done.16) | copy-start | bytes 6148
  54.6 1.8 %copy-start.19 = (f32[1,512]{1,0:T(1,128)S(1)}, f32[1,512]{1,0:T(1,128)}, u32[]{:S(2)}) copy-start(f32[1,512]{1,0:T(1,128)} %copy-done.18) | copy-start | bytes 6148
  54.6 1.8 %copy-start.21 = (f32[1,512]{1,0:T(1,128)S(1)}, f32[1,512]{1,0:T(1,128)}, u32[]{:S(2)}) copy-start(f32[1,512]{1,0:T(1,128)} %copy-done.20) | copy-start | bytes 6148
  54.6 1.8 %copy-start.23 = (f32[1,512]{1,0:T(1,128)S(1)}, f32[1,512]{1,0:T(1,128)}, u32[]{:S(2)}) copy-start(f32[1,512]{1,0:T(1,128)} %copy-done.22) | copy-start | bytes 6148
  54.6 1.8 %copy-start.25 = (f32[1,512]{1,0:T(1,128)S(1)}, f32[1,512]{1,0:T(1,128)}, u32[]{:S(2)}) copy-start(f32[1,512]{1,0:T(1,128)} %copy-done.24) | copy-start | bytes 6148
  54.6 1.8 %copy-start.27 = (f32[1,512]{1,0:T(1,128)S(1)}, f32[1,512]{1,0:T(1,128)}, u32[]{:S(2)}) copy-start(f32[1,512]{1,0:T(1,128)} %copy-done.26) | copy-start | bytes 6148
  58.7 6.3 %collective-permute-start.7 = (bf16[2,128,256]{2,1,0:T(8,128)(2,1)S(1)}, bf16[2,128,256]{2,1,0:T(8,128)(2,1)S(1)}, u32[]{:S(2)}, u32[]{:S(2)}) collective-permute-start(bf16[2,128,256]{2,1,0:T(8,128)(2,1)S(1)} %fusion.7), channel_id=1, source_target_pairs={{0,8},{2,10},{4,12},{6,14},{8,0},{10,2},{12,4},{14,6},{16,24},{18,... | collective-permute-start | bytes 393224 | tf_op jit(solution)/shard_map/ppermute | solution.py:18
  60.4 5.0 %collective-permute-start.8 = (bf16[2,128,256]{2,1,0:T(8,128)(2,1)S(1)}, bf16[2,128,256]{2,1,0:T(8,128)(2,1)S(1)}, u32[]{:S(2)}, u32[]{:S(2)}) collective-permute-start(bf16[2,128,256]{2,1,0:T(8,128)(2,1)S(1)} %fusion.8), channel_id=1, source_target_pairs={{0,4},{2,6},{4,0},{6,2},{8,12},{10,14},{12,8},{14,10},{16,20},{18,... | collective-permute-start | bytes 393224 | tf_op jit(solution)/shard_map/ppermute | solution.py:18
  60.9 1.3 %collective-permute-start.9 = (f32[33,512]{1,0:T(8,128)S(1)}, f32[33,512]{1,0:T(8,128)S(1)}, u32[]{:S(2)}, u32[]{:S(2)}) collective-permute-start(f32[33,512]{1,0:T(8,128)S(1)} %concatenate.16), channel_id=1, source_target_pairs={{0,2},{2,0},{4,6},{6,4},{8,10},{10,8},{12,14},{14,12},{16,18},{18,... | collective-permute-start | bytes 202760 | tf_op jit(solution)/shard_map/ppermute | solution.py:18
  65.3 5.8 %collective-permute-start.11 = (f32[33,512]{1,0:T(8,128)S(1)}, f32[33,512]{1,0:T(8,128)S(1)}, u32[]{:S(2)}, u32[]{:S(2)}) collective-permute-start(f32[33,512]{1,0:T(8,128)S(1)} %add.408), channel_id=1, source_target_pairs={{0,4},{2,6},{4,0},{6,2},{8,12},{10,14},{12,8},{14,10},{16,20},{18,... | collective-permute-start | bytes 202760 | tf_op jit(solution)/shard_map/ppermute | solution.py:18
  66.6 8.3 %collective-permute-start.10 = (bf16[128,512]{1,0:T(8,128)(2,1)S(1)}, bf16[128,512]{1,0:T(8,128)(2,1)S(1)}, u32[]{:S(2)}, u32[]{:S(2)}) collective-permute-start(bf16[128,512]{1,0:T(8,128)(2,1)S(1)} %fusion.9), channel_id=1, source_target_pairs={{0,16},{2,18},{4,20},{6,22},{8,24},{10,26},{12,28},{14,30},{16,0},... | collective-permute-start | bytes 393224 | tf_op jit(solution)/shard_map/ppermute | solution.py:18
  71.0 4.7 %copy-start.7 = (bf16[512,512]{1,0:T(8,128)(2,1)S(1)}, bf16[512,512]{1,0:T(8,128)(2,1)}, u32[]{:S(2)}) copy-start(bf16[512,512]{1,0:T(8,128)(2,1)} %param.9) | copy-start | bytes 1572868
  71.0 4.7 %copy-start.8 = (bf16[512,512]{1,0:T(8,128)(2,1)S(1)}, bf16[512,512]{1,0:T(8,128)(2,1)}, u32[]{:S(2)}) copy-start(bf16[512,512]{1,0:T(8,128)(2,1)} %param.10) | copy-start | bytes 1572868
  75.0 4.5 %collective-permute-start.12 = (f32[33,512]{1,0:T(8,128)S(1)}, f32[33,512]{1,0:T(8,128)S(1)}, u32[]{:S(2)}, u32[]{:S(2)}) collective-permute-start(f32[33,512]{1,0:T(8,128)S(1)} %add.439), channel_id=1, source_target_pairs={{0,8},{2,10},{4,12},{6,14},{8,0},{10,2},{12,4},{14,6},{16,24},{18,... | collective-permute-start | bytes 202760 | tf_op jit(solution)/shard_map/ppermute | solution.py:18
  79.5 6.3 %collective-permute-start.13 = (f32[33,512]{1,0:T(8,128)S(1)}, f32[33,512]{1,0:T(8,128)S(1)}, u32[]{:S(2)}, u32[]{:S(2)}) collective-permute-start(f32[33,512]{1,0:T(8,128)S(1)} %add.440), channel_id=1, source_target_pairs={{0,16},{2,18},{4,20},{6,22},{8,24},{10,26},{12,28},{14,30},{16,0},... | collective-permute-start | bytes 202760 | tf_op jit(solution)/shard_map/ppermute | solution.py:18
  (26 other events, 45.7 us)

commit v2 on v1

v2 whole, which is shorter than its diff:
```python
import jax
import jax.numpy as jnp
import numpy as np
from jax import lax
from jax.experimental import pallas as pl
from jax.experimental.pallas import tpu as pltpu
from jax.sharding import PartitionSpec as P

LANES = 128
TILE = 64


def passed_along(shard, axis, by):
    size = lax.axis_size(axis)
    pairs = [(i, i + by) for i in range(size) if 0 <= i + by < size]
    return lax.ppermute(shard, axis, pairs)


def swapped(shard, axis, bit):
    size = lax.axis_size(axis)
    return lax.ppermute(shard, axis, [(i, i ^ (1 << bit)) for i in range(size)])


def bits_of(size):
    bits = size.bit_length() - 1
    return bits if 1 << bits == size else None


def summed_over(shard, axis):
    bits = bits_of(lax.axis_size(axis))
    if bits is None:
        return lax.psum(shard, axis)
    for bit in range(bits):
        shard = shard + swapped(shard, axis, bit)
    return shard


def together(*values):
    return lax.optimization_barrier(values)


def call(body, outs, *args, scalars=0, scratch=()):
    vmem = pl.BlockSpec(memory_space=pltpu.VMEM)
    return pl.pallas_call(
        body,
        in_specs=[pl.BlockSpec(memory_space=pltpu.SMEM)] * scalars + [vmem] * (len(args) - scalars),
        out_specs=[vmem] * len(outs),
        out_shape=[jax.ShapeDtypeStruct(shape, kind) for shape, kind in outs],
        scratch_shapes=list(scratch),
    )(*args)


def group(g):
    return slice(g * LANES, (g + 1) * LANES)


def as_row(columns):
    return jnp.sum(columns.T, axis=0, keepdims=True)


def as_column(row):
    return jnp.broadcast_to(row, (LANES, row.shape[1])).T


def conv_forward(value, gate, before, conv_taps):
    rows, width = value.shape
    taps = conv_taps.shape[0]
    pad = before.shape[0]
    groups = width // LANES

    def body(value_ref, gate_ref, before_ref, taps_ref, conv_ref, padded_ref, sums_ref):
        for g in range(groups):
            padded_ref[g, :pad, :] = before_ref[:, group(g)].astype(jnp.float32)
            v = value_ref[:, group(g)].astype(jnp.float32)
            s = jax.nn.sigmoid(gate_ref[:, group(g)].astype(jnp.float32))
            padded_ref[g, pad:, :] = (v * s).astype(jnp.bfloat16).astype(jnp.float32)
        for g in range(groups):
            weights = [taps_ref[k : k + 1, group(g)] for k in range(taps)]

            def tile(n, carry):
                first = pl.multiple_of(n * TILE, TILE)
                total = jnp.zeros((TILE, LANES), jnp.float32)
                for k in range(taps):
                    total = total + weights[k] * padded_ref[
                        g, pl.ds(first + (pad - taps + 1 + k), TILE), :
                    ]
                conv_ref[pl.ds(first, TILE), group(g)] = total
                return carry

            lax.fori_loop(0, rows // TILE, tile, 0)
        total = jnp.zeros((rows, LANES), jnp.float32)
        squares = jnp.zeros((rows, LANES), jnp.float32)
        for g in range(groups):
            c = conv_ref[:, group(g)]
            total = total + c
            squares = squares + c * c
        sums_ref[0:1, :] = as_row(total)
        sums_ref[1:2, :] = as_row(squares)

    return call(
        body,
        [
            ((rows, width), jnp.float32),
            ((groups, rows + pad, LANES), jnp.float32),
            ((2, rows), jnp.float32),
        ],
        value, gate, before, conv_taps,
    )


def statistics(sums_ref, channels):
    mean = sums_ref[0:1, :] / channels
    var = sums_ref[1:2, :] / channels - mean * mean
    return as_column(mean), as_column(lax.rsqrt(var + 1e-05))


def products(me_ref, order, grad_ref, act, block):
    for n in range(0, len(order), 2):
        picked = [
            grad_ref[:, pl.ds(pl.multiple_of((me_ref[0] ^ b) * block, block), block)]
            for b in order[n : n + 2]
        ]
        pair = jnp.dot(
            act, jnp.concatenate(picked, axis=1), preferred_element_type=jnp.float32
        )
        yield n, pair[:, :block]
        yield n + 1, pair[:, block:]


def normed_act(conv, sums, gain, bias, out_grad, me, order, block, channels):
    rows, width = conv.shape
    groups = width // LANES
    count = len(order)

    def body(me_ref, conv_ref, sums_ref, gain_ref, bias_ref, grad_ref, act_ref, sent_ref):
        mean, rstd = statistics(sums_ref, channels)
        for g in range(groups):
            xhat = (conv_ref[:, group(g)] - mean) * rstd
            normed = xhat * gain_ref[:, group(g)] + bias_ref[:, group(g)]
            act = normed * jax.nn.sigmoid(normed)
            act_ref[group(g), :] = act.T.astype(jnp.bfloat16)
        if count:
            for n, product in products(me_ref, order, grad_ref, act_ref[...], block):
                sent_ref[n] = product.astype(jnp.bfloat16)
        else:
            sent_ref[...] = jnp.zeros_like(sent_ref)

    shape = (count, width, block) if count else (16, LANES)
    return call(
        body,
        [((width, rows), jnp.bfloat16), (shape, jnp.bfloat16)],
        me, conv, sums, gain, bias, out_grad,
        scalars=1,
    )


def kept_products(act, out_grad, me, order, block, got):
    width = act.shape[0]
    half = width // 2
    count = len(order)

    def body(me_ref, act_ref, grad_ref, got_ref, kl_ref, sl_ref, kr_ref, sr_ref):
        for n, product in products(me_ref, order, grad_ref, act_ref[...], block):
            product = product + got_ref[n].astype(jnp.float32)
            left, right = product[:half], product[half:]
            first, second, rest = n >> 2, (n >> 1) & 1, n & 1
            if first:
                sl_ref[second * 2 + rest] = left.astype(jnp.bfloat16)
            else:
                kl_ref[second * 2 + rest] = left
            if second:
                sr_ref[first * 2 + rest] = right.astype(jnp.bfloat16)
            else:
                kr_ref[first * 2 + rest] = right

    shape = (count // 2, half, block)
    return call(
        body,
        [(shape, jnp.float32), (shape, jnp.bfloat16)] * 2,
        me, act, out_grad, got,
        scalars=1,
    )


def normed_gradient(conv, sums, gain, bias, upper, lower, channels):
    rows, width = conv.shape
    groups = width // LANES
    cut = upper.shape[0]

    def body(conv_ref, sums_ref, gain_ref, bias_ref, up_ref, low_ref, gx_ref, xhat_ref, row_ref, col_ref):
        mean, rstd = statistics(sums_ref, channels)
        first = jnp.zeros((rows, LANES), jnp.float32)
        second = jnp.zeros((rows, LANES), jnp.float32)
        for g in range(groups):
            xhat = (conv_ref[:, group(g)] - mean) * rstd
            normed = xhat * gain_ref[:, group(g)] + bias_ref[:, group(g)]
            sig = jax.nn.sigmoid(normed)
            ga = jnp.concatenate([up_ref[:, group(g)], low_ref[:, group(g)]], axis=0)
            gn = ga * sig * (1.0 + normed * (1.0 - sig))
            col_ref[0:1, group(g)] = jnp.sum(gn * xhat, axis=0, keepdims=True)
            col_ref[1:2, group(g)] = jnp.sum(gn, axis=0, keepdims=True)
            gx = gn * gain_ref[:, group(g)]
            first = first + gx
            second = second + gx * xhat
            gx_ref[:, group(g)] = gx
            xhat_ref[:, group(g)] = xhat
        row_ref[0:1, :] = as_row(first)
        row_ref[1:2, :] = as_row(second)

    return call(
        body,
        [
            ((rows, width), jnp.float32),
            ((rows, width), jnp.float32),
            ((2, rows), jnp.float32),
            ((2, width), jnp.float32),
        ],
        conv, sums, gain, bias, upper, lower,
    )


def conv_gradient(gx, xhat, sums, terms, channels, pad):
    rows, width = gx.shape
    groups = width // LANES

    def body(gx_ref, xhat_ref, sums_ref, terms_ref, out_ref, edge_ref):
        _, rstd = statistics(sums_ref, channels)
        first = as_column(terms_ref[0:1, :] / channels)
        second = as_column(terms_ref[1:2, :] / channels)
        for g in range(groups):
            out = rstd * (gx_ref[:, group(g)] - first - xhat_ref[:, group(g)] * second)
            out_ref[g] = out
            edge_ref[g] = out[:pad]

    return call(
        body,
        [((groups, rows, LANES), jnp.float32), ((groups, pad, LANES), jnp.float32)],
        gx, xhat, sums, terms,
    )


def taps_gradient(grad_conv, padded, columns, taps):
    groups, rows, _ = grad_conv.shape
    pad = padded.shape[1] - rows
    height = -(-(taps + 2) // 8) * 8

    def body(grad_ref, padded_ref, col_ref, out_ref):
        out_ref[...] = jnp.zeros_like(out_ref)
        out_ref[taps : taps + 2, :] = col_ref[...]
        for g in range(groups):
            def tile(n, totals):
                first = pl.multiple_of(n * 16, 16)
                grad = [grad_ref[g, pl.ds(first + 8 * m, 8), :] for m in range(2)]
                return tuple(
                    totals[k] + sum(
                        grad[m] * padded_ref[g, pl.ds(first + (8 * m + pad - taps + 1 + k), 8), :]
                        for m in range(2)
                    )
                    for k in range(taps)
                )

            totals = lax.fori_loop(
                0, rows // 16, tile, tuple(jnp.zeros((8, LANES), jnp.float32) for _ in range(taps))
            )
            for k in range(taps):
                out_ref[k : k + 1, group(g)] = jnp.sum(totals[k], axis=0, keepdims=True)

    return call(body, [((height, groups * LANES), jnp.float32)], grad_conv, padded, columns)[0]


def conv_backward(grad_conv, ahead, conv_taps, value, gate, start):
    groups, rows, _ = grad_conv.shape
    taps = conv_taps.shape[0]
    count = rows // 2
    width = groups * LANES
    final = ahead is not None

    def body(*refs):
        if final:
            grad_ref, ahead_ref, taps_ref, value_ref, gate_ref, gv_ref, gg_ref, held_ref = refs
            held_ref[:, :count, :] = grad_ref[:, start:, :]
            held_ref[:, count:, :] = ahead_ref[...]
            source, base = held_ref, 0
        else:
            grad_ref, taps_ref, value_ref, gate_ref, gv_ref, gg_ref = refs
            source, base = grad_ref, start
        for g in range(groups):
            weights = [taps_ref[k : k + 1, group(g)] for k in range(taps)]

            def tile(n, carry):
                first = pl.multiple_of(n * TILE, TILE)
                total = jnp.zeros((TILE, LANES), jnp.float32)
                for k in range(taps):
                    total = total + weights[k] * source[
                        g, pl.ds(first + (base + taps - 1 - k), TILE), :
                    ]
                here = pl.ds(first + start, TILE)
                v = value_ref[here, group(g)].astype(jnp.float32)
                s = jax.nn.sigmoid(gate_ref[here, group(g)].astype(jnp.float32))
                gv_ref[pl.ds(first, TILE), group(g)] = (total * s).astype(jnp.bfloat16)
                gg_ref[pl.ds(first, TILE), group(g)] = (total * v * s * (1.0 - s)).astype(jnp.bfloat16)
                return carry

            lax.fori_loop(0, count // TILE, tile, 0)

    outs = [((count, width), jnp.bfloat16)] * 2
    if final:
        scratch = [pltpu.VMEM((groups, count + ahead.shape[1], LANES), jnp.float32)]
        return call(body, outs, grad_conv, ahead, conv_taps, value, gate, scratch=scratch)
    return call(body, outs, grad_conv, conv_taps, value, gate)


def halved(blocks, axis, bit):
    count = blocks.shape[0] // 2
    return blocks[:count], swapped(blocks[count:].astype(jnp.bfloat16), axis, bit)


def added(pair):
    return pair[0] + pair[1].astype(jnp.float32)


def on_device(
    glu_value, glu_gate, conv_taps, channel_norm_gain, channel_norm_bias, out_proj, out_grad
):
    rows, width = glu_value.shape
    taps = conv_taps.shape[0]
    pad = -(-(taps - 1) // 16) * 16
    channels = width * lax.axis_size("tp")
    size = lax.axis_size("sp")
    bits = bits_of(size)
    block = out_grad.shape[1] // size
    by_halves = bits == 4 and block % LANES == 0 and width % 256 == 0
    gain, bias = channel_norm_gain[None, :], channel_norm_bias[None, :]
    cut = rows // 2
    me = lax.axis_index("sp").astype(jnp.int32).reshape(1)
    relative = []
    if by_halves:
        relative = [
            sum(((n >> (bits - 2 - b)) & 1) << (b + 1) for b in range(bits - 1))
            for n in range(size // 2)
        ]

    edge = (
        glu_value[rows - pad :].astype(jnp.float32)
        * jax.nn.sigmoid(glu_gate[rows - pad :].astype(jnp.float32))
    ).astype(jnp.bfloat16)
    before = passed_along(edge, "sp", 1)

    def act_gradient(part):
        return lax.dot_general(
            part, out_proj, (((1,), (1,)), ((), ())), preferred_element_type=jnp.float32
        )

    upper = act_gradient(out_grad[:cut])
    before, upper = together(before, upper)
    conv, padded, sums = conv_forward(glu_value, glu_gate, before, conv_taps)
    later, sums = together(out_grad, sums)
    lower = act_gradient(later[cut:])
    sums = summed_over(sums, "tp")
    sums, lower = together(sums, lower)
    act, sent = normed_act(
        conv, sums, gain, bias, out_grad, me, [r + 1 for r in relative], block, channels
    )
    if by_halves:
        got = swapped(sent, "sp", 0)
        sums, act = together(sums, act)
    gx, xhat, row_terms, column_terms = normed_gradient(
        conv, sums, gain, bias, upper, lower, channels
    )
    terms = summed_over(row_terms, "tp")
    if by_halves:
        got, row_terms = together(got, row_terms)
        kl, sl, kr, sr = kept_products(act, out_grad, me, relative, block, got)
        left = (kl, swapped(sl, "sp", 1))
        right = (kr, swapped(sr, "sp", 2))
        terms, kl = together(terms, kl)
        left = (kl, left[1])
    else:
        grad_proj = lax.psum_scatter(
            lax.dot_general(
                out_grad, act, (((0,), (1,)), ((), ())), preferred_element_type=jnp.float32
            ),
            "sp",
            scatter_dimension=0,
            tiled=True,
        )
    grad_conv, edge_gradient = conv_gradient(gx, xhat, sums, terms, channels, pad)
    ahead = passed_along(edge_gradient, "sp", -1)
    summed = taps_gradient(grad_conv, padded, column_terms, taps)
    if by_halves:
        left, right, summed, grad_conv = together(left, right, summed, grad_conv)
        left = halved(added(left), "sp", 2)
        right = halved(added(right), "sp", 1)
        summed = (summed, swapped(summed, "sp", 0))
    top = conv_backward(grad_conv, None, conv_taps, glu_value, glu_gate, 0)
    if by_halves:
        left, right, summed, top, grad_conv = together(left, right, summed, top, grad_conv)
        both = jnp.concatenate([added(left), added(right)], axis=1)
        both = halved(both, "sp", 3)
        summed = summed[0] + summed[1]
        summed = (summed, swapped(summed, "sp", 1))
    bottom = conv_backward(grad_conv, ahead, conv_taps, glu_value, glu_gate, cut)
    if by_halves:
        both, summed, bottom = together(both, summed, bottom)
        grad_proj = added(both)[0].T
        summed = summed[0] + summed[1]
        for bit in (2, 3):
            summed = summed + swapped(summed, "sp", bit)
    else:
        summed = summed_over(summed, "sp")
    grad_value = jnp.concatenate([top[0], bottom[0]], axis=0)
    grad_gate = jnp.concatenate([top[1], bottom[1]], axis=0)
    return (grad_value, grad_gate, summed[:taps], summed[taps], summed[taps + 1], grad_proj)


def solution(mesh):
    return jax.shard_map(
        on_device,
        mesh=mesh,
        in_specs=(
            P("sp", "tp"),
            P("sp", "tp"),
            P(None, "tp"),
            P("tp"),
            P("tp"),
            P("tp", None),
            P("sp", None),
        ),
        out_specs=(P("sp", "tp"), P("sp", "tp"), P(None, "tp"), P("tp"), P("tp"), P("sp", "tp")),
        check_vma=False,
    )
```

time: 87.6 us -> 80.6 us (0.920)
  Pallas kernels: 7.26 us -> 33.6 us
  other arithmetic: 27.5 us -> 8.74 us
  waiting for transfers between devices: 15.3 us -> 6.03 us
  local copies, waits for them, and re-layouts: 10.5 us -> 4.39 us
  matrix products: 3.87 us -> 5.54 us
  between operations: 2.02 us -> 0.83 us
    pallas_call x2 -> x8, Pallas kernels: 7.26 us -> 33.6 us  [call(): pl.pallas_call(body, in_specs=[pl.BlockSpec(memory_space=pltpu.SMEM)] * s...]
    reduce_sum x4 -> x0, other arithmetic: 13.7 us -> none  [the longest x2 6.17 us: on_device(): jnp.sum(conv_output_gradient * padded[k:k + rows], axis=0)]
    ppermute x12, waiting for transfers between devices: 15.2 us -> 6.03 us  [swapped(): return lax.ppermute(shard, axis, [(i, i ^ 1 << bit) for i in range(size)])]
    add x2 -> x0, other arithmetic: 4.09 us -> none  [conv_back(): total + conv_taps[k][None, :] * source[taps - 1 - k:taps - 1 - k + count]]
    concatenate x2 -> x0, local copies, waits for them, and re-layouts: 3.72 us -> none  [the longest x1 3.68 us: on_device(): summed = jnp.concatenate([taps_local, column_terms], axis=0)]
    convert_element_type x4 -> x1, other arithmetic: 4.26 us -> 0.96 us  [on_device(): edge = (glu_value[rows - pad:].astype(jnp.float32) * jax.nn.sigmoid(glu_g...]
    add x6 -> x4, other arithmetic: 4.16 us -> 1.12 us  [added(): return pair[0] + pair[1].astype(jnp.float32)]
    slice x4, local copies, waits for them, and re-layouts: 2.81 us -> 0.08 us  [the longest x2 0.04 us: halved(): blocks[count:].astype(jnp.bfloat16)]
  transfers between devices with their start and end apart: 14 -> 14, of which waited for: 8 -> 3; matrix products, arithmetic and copies ran while one was open for 18% -> 15% of each run, Pallas kernels for 4% -> 25%
where the time goes in v2:
time: 80.6 us; the launch traced here: 80.1 us
  Pallas kernels  33.6 us (42%)
  starting transfers between devices  20.9 us (26%)
  other arithmetic  8.74 us (11%)
  waiting for transfers between devices  6.03 us (7%)
  matrix products  5.54 us (7%)
  local copies, waits for them, and re-layouts  4.39 us (5%)
  between operations  0.83 us (1%)
    pallas_call x8, Pallas kernels, call(): pl.pallas_call(body, in_specs=[pl.BlockSpec(memory_space=pltpu.SMEM)] * s...  33.6 us
    ppermute x12, starting transfers between devices, swapped(): return lax.ppermute(shard, axis, [(i, i ^ 1 << bit) for i in range(size)])  17.2 us
    ppermute x12, waiting for transfers between devices, swapped(): return lax.ppermute(shard, axis, [(i, i ^ 1 << bit) for i in range(size)])  6.03 us
    dot_general x2, matrix products, act_gradient(): lax.dot_general(part, out_proj, (((1,), (1,)), ((), ())), preferred_eleme...  5.54 us
    ppermute x2, starting transfers between devices, passed_along(): return lax.ppermute(shard, axis, pairs)  3.68 us
    unnamed x25, local copies, waits for them, and re-layouts  3.1 us
    concatenate x1, other arithmetic, on_device(): grad_value = jnp.concatenate([top[0], bottom[0]], axis=0)  1.98 us
    add x2, other arithmetic, on_device(): summed = summed[0] + summed[1]  1.83 us
  transfers between devices with their start and end apart: 14, of which 3 were waited for; matrix products, arithmetic and copies ran while one was open for 15% of the time, Pallas kernels for 25%

profile of v2, /device:TPU:0, one launch (start us, length us, event | category | flops | bytes accessed | tf_op | source)
XLA Modules:
  0.0 80.1 jit_solution(17312512147516938792)
XLA Ops:
  0.6 0.0 copy-start
  0.6 1.0 %multiply_convert_fusion = bf16[32,512]{1,0:T(8,128)(2,1)S(1)} fusion(bf16[512,512]{1,0:T(8,128)(2,1)} %refs_4_.1, bf16[512,512]{1,0:T(8,128)(2,1)} %refs_3_.3), kind=kLoop, calls=%fused_computation.18 | loop fusion | flops 114688 | bytes 98304 | tf_op jit(solution)/shard_map/convert_element_type | solution.py:346
  1.6 2.4 %collective-permute-start = (bf16[32,512]{1,0:T(8,128)(2,1)S(1)}, bf16[32,512]{1,0:T(8,128)(2,1)S(1)}, u32[]{:S(2)}, u32[]{:S(2)}) collective-permute-start(bf16[32,512]{1,0:T(8,128)(2,1)S(1)} %multiply_convert_fusion), channel_id=1, source_target_pairs={{0,2},{2,4},{4,6},{6,8},{8,10},{10,12},{12,14},{14,16},{16,18},{18... | collective-permute-start | bytes 98312 | tf_op jit(solution)/shard_map/ppermute | solution.py:16
  4.0 0.0 copy-done
  4.0 2.8 %fusion.2.up_ref = f32[256,512]{1,0:T(8,128)} fusion(bf16[512,2048]{1,0:T(8,128)(2,1)S(1)} %copy-done, bf16[512,2048]{1,0:T(8,128)(2,1)} %grad_ref.3), kind=kOutput, calls=%fused_computation.2 | convolution fusion | flops 536870912 | bytes 3670016 | tf_op jit(solution)/shard_map/dot_general | solution.py:350
  6.8 0.0 collective-permute-done.before_ref
  6.8 0.6 copy-done.9
  7.4 5.4 %shard_map.118 = (f32[512,512]{1,0:T(8,128)}, f32[4,544,128]{2,1,0:T(8,128)}, f32[2,512]{1,0:T(2,128)}) custom-call(bf16[512,512]{1,0:T(8,128)(2,1)} %refs_3_.3, bf16[512,512]{1,0:T(8,128)(2,1)} %refs_4_.1, bf16[32,512]{1,0:T(8,128)(2,1)} %copy-done.9, f32[31,512]{1,0:T(8,128)} %refs_2_.3), custom_call_target="tpu_custom_call" | custom-call | tf_op jit(solution)/shard_map/pallas_call | solution.py:44
  12.9 2.3 %collective-permute-start.1 = (f32[2,512]{1,0:T(2,128)}, f32[2,512]{1,0:T(2,128)S(1)}, u32[]{:S(2)}, u32[]{:S(2)}) collective-permute-start(f32[2,512]{1,0:T(2,128)} %get-tuple-element.60), channel_id=1, source_target_pairs={{0,1},{1,0},{2,3},{3,2},{4,5},{5,4},{6,7},{7,6},{8,9},{9,8},{10,11... | collective-permute-start | bytes 12296 | tf_op jit(solution)/shard_map/ppermute | solution.py:21
  15.2 2.8 %fusion.low_ref = f32[256,512]{1,0:T(8,128)} fusion(bf16[512,2048]{1,0:T(8,128)(2,1)S(1)} %copy-done, bf16[512,2048]{1,0:T(8,128)(2,1)} %grad_ref.3), kind=kOutput, calls=%fused_computation | convolution fusion | flops 536870912 | bytes 3670016 | tf_op jit(solution)/shard_map/dot_general | solution.py:350
  17.9 0.0 collective-permute-done.1
  17.9 0.0 copy-done.11
  17.9 0.6 add.37.sums_ref
  18.5 4.1 %shard_map.119 = (bf16[512,512]{1,0:T(8,128)(2,1)}, bf16[8,512,128]{2,1,0:T(8,128)(2,1)}) custom-call(s32[1]{0:T(128)} %bitcast.me_ref, f32[512,512]{1,0:T(8,128)} %get-tuple-element.58.conv_ref, f32[2,512]{1,0:T(2,128)} %add.37.sums_ref, f32[1,512]{1,0:T(1,128)} %bitcast.11, f32[1,512]{1,0:T(1,128)} %bitcast.13, bf16[512,2048]{1,0:T(8,128)(2,1)} %grad_ref.3), custom_call_target="tpu_custom_call" | custom-call | tf_op jit(solution)/shard_map/pallas_call | solution.py:44
  22.6 1.5 %collective-permute-start.3 = (bf16[8,512,128]{2,1,0:T(8,128)(2,1)}, bf16[8,512,128]{2,1,0:T(8,128)(2,1)S(1)}, u32[]{:S(2)}, u32[]{:S(2)}) collective-permute-start(bf16[8,512,128]{2,1,0:T(8,128)(2,1)} %get-tuple-element.69), channel_id=1, source_target_pairs={{0,2},{2,0},{4,6},{6,4},{8,10},{10,8},{12,14},{14,12},{16,18},{18,... | collective-permute-start | bytes 3145736 | tf_op jit(solution)/shard_map/ppermute | solution.py:21
  24.1 3.5 %shard_map.120 = (f32[512,512]{1,0:T(8,128)}, f32[512,512]{1,0:T(8,128)}, f32[2,512]{1,0:T(2,128)}, f32[2,512]{1,0:T(2,128)}) custom-call(f32[512,512]{1,0:T(8,128)} %get-tuple-element.58.conv_ref, f32[2,512]{1,0:T(2,128)} %add.37.sums_ref, f32[1,512]{1,0:T(1,128)} %bitcast.12, f32[1,512]{1,0:T(1,128)} %bitcast.14, f32[256,512]{1,0:T(8,128)} %fusion.2.up_ref, ...), custom_call_target="tpu_custom_call" | custom-call | tf_op jit(solution)/shard_map/pallas_call | solution.py:44
  27.6 0.0 collective-permute-done.3.got_ref
  27.6 0.0 copy-start.1
  27.6 1.0 %copy-done.1 = bf16[8,512,128]{2,1,0:T(8,128)(2,1)} copy-done((bf16[8,512,128]{2,1,0:T(8,128)(2,1)}, bf16[8,512,128]{2,1,0:T(8,128)(2,1)S(1)}, u32[]{:S(2)}) %copy-start.1) | copy-done | bytes 1048600
  28.6 3.7 %shard_map.121 = (f32[4,256,128]{2,1,0:T(8,128)}, bf16[4,256,128]{2,1,0:T(8,128)(2,1)}, f32[4,256,128]{2,1,0:T(8,128)}, bf16[4,256,128]{2,1,0:T(8,128)(2,1)}) custom-call(s32[1]{0:T(128)} %bitcast.me_ref, bf16[512,512]{1,0:T(8,128)(2,1)} %get-tuple-element.68.act_ref, bf16[512,2048]{1,0:T(8,128)(2,1)} %grad_ref.3, bf16[8,512,128]{2,1,0:T(8,128)(2,1)} %copy-done.1), custom_call_target="tpu_custom_call" | custom-call | tf_op jit(solution)/shard_map/pallas_call | solution.py:44
  32.4 1.5 %collective-permute-start.4 = (bf16[4,256,128]{2,1,0:T(8,128)(2,1)}, bf16[4,256,128]{2,1,0:T(8,128)(2,1)}, u32[]{:S(2)}, u32[]{:S(2)}) collective-permute-start(bf16[4,256,128]{2,1,0:T(8,128)(2,1)} %get-tuple-element.73), channel_id=1, source_target_pairs={{0,4},{2,6},{4,0},{6,2},{8,12},{10,14},{12,8},{14,10},{16,20},{18,... | collective-permute-start | bytes 786440 | tf_op jit(solution)/shard_map/ppermute | solution.py:21
  33.9 1.6 %collective-permute-start.5 = (bf16[4,256,128]{2,1,0:T(8,128)(2,1)}, bf16[4,256,128]{2,1,0:T(8,128)(2,1)S(1)}, u32[]{:S(2)}, u32[]{:S(2)}) collective-permute-start(bf16[4,256,128]{2,1,0:T(8,128)(2,1)} %get-tuple-element.75), channel_id=1, source_target_pairs={{0,8},{2,10},{4,12},{6,14},{8,0},{10,2},{12,4},{14,6},{16,24},{18,... | collective-permute-start | bytes 786440 | tf_op jit(solution)/shard_map/ppermute | solution.py:21
  35.4 0.0 copy-done.10
  35.4 0.5 collective-permute-start.2
  36.0 3.1 %collective-permute-done.2 = f32[2,512]{1,0:T(2,128)S(1)} collective-permute-done((f32[2,512]{1,0:T(2,128)S(1)}, f32[2,512]{1,0:T(2,128)S(1)}, u32[]{:S(2)}, u32[]{:S(2)}) %collective-permute-start.2) | collective-permute-done | bytes 4128 | tf_op jit(solution)/shard_map/ppermute | solution.py:21
  39.1 0.6 add.38.terms_ref
  39.6 3.0 %shard_map.122 = (f32[4,512,128]{2,1,0:T(8,128)}, f32[4,32,128]{2,1,0:T(8,128)}) custom-call(f32[512,512]{1,0:T(8,128)} %get-tuple-element.76.gx_ref, f32[512,512]{1,0:T(8,128)} %get-tuple-element.77.xhat_ref, f32[2,512]{1,0:T(2,128)} %add.37.sums_ref, f32[2,512]{1,0:T(2,128)} %add.38.terms_ref), custom_call_target="tpu_custom_call" | custom-call | tf_op jit(solution)/shard_map/pallas_call | solution.py:44
  42.6 5.9 %shard_map.123 = f32[40,512]{1,0:T(8,128)} custom-call(f32[4,512,128]{2,1,0:T(8,128)} %get-tuple-element.97.grad_ref.refs_0_, f32[4,544,128]{2,1,0:T(8,128)} %get-tuple-element.80.padded_ref, f32[2,512]{1,0:T(2,128)} %get-tuple-element.81.col_ref), custom_call_target="tpu_custom_call" | custom-call | tf_op jit(solution)/shard_map/pallas_call | solution.py:44
  48.5 0.0 collective-permute-done.4
  48.5 0.0 collective-permute-done.5
  48.5 0.0 copy-done.3
  48.5 1.0 %convert_add_fusion.1 = f32[4,256,128]{2,1,0:T(8,128)S(1)} fusion(f32[4,256,128]{2,1,0:T(8,128)S(1)} %copy-done.3, bf16[4,256,128]{2,1,0:T(8,128)(2,1)} %collective-permute-done.4), kind=kLoop, calls=%fused_computation.9 | loop fusion | flops 262144 | bytes 1310720 | tf_op jit(solution)/shard_map/add | solution.py:319
  49.6 0.5 collective-permute-start.6
  50.1 0.0 copy-done.2
  50.2 0.6 collective-permute-start.7
  50.7 0.0 copy-done.4
  50.7 0.0 collective-permute-start.8
  50.7 1.3 %collective-permute-start.11 = (f32[4,32,128]{2,1,0:T(8,128)}, f32[4,32,128]{2,1,0:T(8,128)S(1)}, u32[]{:S(2)}, u32[]{:S(2)}) collective-permute-start(f32[4,32,128]{2,1,0:T(8,128)} %get-tuple-element.98), channel_id=1, source_target_pairs={{2,0},{4,2},{6,4},{8,6},{10,8},{12,10},{14,12},{16,14},{18,16},{20... | collective-permute-start | bytes 196616 | tf_op jit(solution)/shard_map/ppermute | solution.py:16
  52.1 4.0 %shard_map.124 = (bf16[256,512]{1,0:T(8,128)(2,1)}, bf16[256,512]{1,0:T(8,128)(2,1)}) custom-call(f32[4,512,128]{2,1,0:T(8,128)} %get-tuple-element.97.grad_ref.refs_0_, f32[31,512]{1,0:T(8,128)} %refs_2_.3, bf16[512,512]{1,0:T(8,128)(2,1)} %refs_3_.3, bf16[512,512]{1,0:T(8,128)(2,1)} %refs_4_.1), custom_call_target="tpu_custom_call" | custom-call | tf_op jit(solution)/shard_map/pallas_call | solution.py:44
  56.1 0.0 collective-permute-done.8
  56.1 0.0 collective-permute-done.6
  56.1 0.0 collective-permute-done.7
  56.1 0.7 fusion.5
  56.8 4.7 %collective-permute-start.9 = (bf16[1,512,128]{2,1,0:T(8,128)(2,1)}, bf16[1,512,128]{2,1,0:T(8,128)(2,1)}, u32[]{:S(2)}, u32[]{:S(2)}) collective-permute-start(bf16[1,512,128]{2,1,0:T(8,128)(2,1)} %fusion.5), channel_id=1, source_target_pairs={{0,16},{2,18},{4,20},{6,22},{8,24},{10,26},{12,28},{14,30},{16,0},... | collective-permute-start | bytes 393224 | tf_op jit(solution)/shard_map/ppermute | solution.py:21
  61.5 0.9 %add.43 = f32[40,512]{1,0:T(8,128)S(1)} add(f32[40,512]{1,0:T(8,128)S(1)} %copy-done.4, f32[40,512]{1,0:T(8,128)} %collective-permute-done.8) | non-fusion elementwise | flops 20480 | bytes 245760 | tf_op jit(solution)/shard_map/add | solution.py:400
  62.4 0.0 copy-start.5
  62.4 0.0 copy-start.6
  62.4 0.8 collective-permute-start.10
  63.2 0.0 collective-permute-done.11.refs_1_
  63.2 0.6 copy-done.8
  63.9 4.1 %shard_map.125 = (bf16[256,512]{1,0:T(8,128)(2,1)}, bf16[256,512]{1,0:T(8,128)(2,1)}) custom-call(f32[4,512,128]{2,1,0:T(8,128)} %get-tuple-element.97.grad_ref.refs_0_, f32[4,32,128]{2,1,0:T(8,128)} %copy-done.8, f32[31,512]{1,0:T(8,128)} %refs_2_.3, bf16[512,512]{1,0:T(8,128)(2,1)} %refs_3_.3, bf16[512,512]{1,0:T(8,128)(2,1)} %refs_4_.1), custom_call_target="tpu_custom_call" | custom-call | tf_op jit(solution)/shard_map/pallas_call | solution.py:44
  67.9 0.0 collective-permute-done.10
  68.0 0.0 collective-permute-done.9
  68.0 0.9 %add.44 = f32[40,512]{1,0:T(8,128)S(1)} add(f32[40,512]{1,0:T(8,128)S(1)} %add.43, f32[40,512]{1,0:T(8,128)} %collective-permute-done.10) | non-fusion elementwise | flops 20480 | bytes 245760 | tf_op jit(solution)/shard_map/add | solution.py:406
  68.9 1.7 %collective-permute-start.12 = (f32[40,512]{1,0:T(8,128)S(1)}, f32[40,512]{1,0:T(8,128)S(1)}, u32[]{:S(2)}, u32[]{:S(2)}) collective-permute-start(f32[40,512]{1,0:T(8,128)S(1)} %add.44), channel_id=1, source_target_pairs={{0,8},{2,10},{4,12},{6,14},{8,0},{10,2},{12,4},{14,6},{16,24},{18,... | collective-permute-start | bytes 245768 | tf_op jit(solution)/shard_map/ppermute | solution.py:21
  70.6 0.9 %add_bitcast_fusion = f32[128,512]{0,1:T(8,128)S(1)} fusion(f32[1,512,128]{2,1,0:T(8,128)S(1)} %fusion.4, bf16[1,512,128]{2,1,0:T(8,128)(2,1)} %collective-permute-done.9), kind=kLoop, calls=%fused_computation.15 | loop fusion | flops 131072 | bytes 655360 | tf_op jit(solution)/shard_map/transpose | solution.py:405
  71.5 0.8 %copy.13 = f32[128,512]{1,0:T(8,128)} copy(f32[128,512]{0,1:T(8,128)S(1)} %add_bitcast_fusion) | data formatting | bytes 524288
  72.3 1.1 %collective-permute-done.12 = f32[40,512]{1,0:T(8,128)S(1)} collective-permute-done((f32[40,512]{1,0:T(8,128)S(1)}, f32[40,512]{1,0:T(8,128)S(1)}, u32[]{:S(2)}, u32[]{:S(2)}) %collective-permute-start.12) | collective-permute-done | bytes 81952 | tf_op jit(solution)/shard_map/ppermute | solution.py:21
  73.4 1.6 %collective-permute-start.13 = (f32[40,512]{1,0:T(8,128)S(1)}, f32[40,512]{1,0:T(8,128)S(1)}, u32[]{:S(2)}, u32[]{:S(2)}) collective-permute-start(f32[40,512]{1,0:T(8,128)S(1)} %add.45), channel_id=1, source_target_pairs={{0,16},{2,18},{4,20},{6,22},{8,24},{10,26},{12,28},{14,30},{16,0},... | collective-permute-start | bytes 245768 | tf_op jit(solution)/shard_map/ppermute | solution.py:21
  75.0 0.0 copy-done.5
  75.0 2.0 %pad_maximum_fusion = (bf16[512,512]{1,0:T(8,128)(2,1)}, bf16[512,512]{1,0:T(8,128)(2,1)}) fusion(bf16[256,512]{1,0:T(8,128)(2,1)S(1)} %copy-done.7, bf16[256,512]{1,0:T(8,128)(2,1)S(1)} %copy-done.5, bf16[256,512]{1,0:T(8,128)(2,1)} %get-tuple-element.103, bf16[256,512]{1,0:T(8,128)(2,1)S(1)} %copy-done.6), kind=kLoop, calls=%fused_computation.6 | loop fusion | flops 2097152 | bytes 2097152 | tf_op jit(solution)/shard_map/concatenate | solution.py:411
  77.0 1.9 %collective-permute-done.13 = f32[40,512]{1,0:T(8,128)S(1)} collective-permute-done((f32[40,512]{1,0:T(8,128)S(1)}, f32[40,512]{1,0:T(8,128)S(1)}, u32[]{:S(2)}, u32[]{:S(2)}) %collective-permute-start.13) | collective-permute-done | bytes 81952 | tf_op jit(solution)/shard_map/ppermute | solution.py:21
  78.8 0.6 fusion.6
  79.4 0.6 slice.61
  (20 shorter events, 0.2 us)
Async XLA Ops:
  0.6 3.4 %copy-start = (bf16[512,2048]{1,0:T(8,128)(2,1)S(1)}, bf16[512,2048]{1,0:T(8,128)(2,1)}, u32[]{:S(2)}) copy-start(bf16[512,2048]{1,0:T(8,128)(2,1)} %param.12) | copy-start | bytes 6291460
  1.6 5.2 %collective-permute-start = (bf16[32,512]{1,0:T(8,128)(2,1)S(1)}, bf16[32,512]{1,0:T(8,128)(2,1)S(1)}, u32[]{:S(2)}, u32[]{:S(2)}) collective-permute-start(bf16[32,512]{1,0:T(8,128)(2,1)S(1)} %multiply_convert_fusion), channel_id=1, source_target_pairs={{0,2},{2,4},{4,6},{6,8},{8,10},{10,12},{12,14},{14,16},{16,18},{18... | collective-permute-start | bytes 98312 | tf_op jit(solution)/shard_map/ppermute | solution.py:16
  6.8 0.6 copy-start.9
  12.9 5.1 %copy-start.11 = (f32[2,512]{1,0:T(2,128)S(1)}, f32[2,512]{1,0:T(2,128)}, u32[]{:S(2)}) copy-start(f32[2,512]{1,0:T(2,128)} %get-tuple-element.60) | copy-start | bytes 12292
  12.9 5.1 %collective-permute-start.1 = (f32[2,512]{1,0:T(2,128)}, f32[2,512]{1,0:T(2,128)S(1)}, u32[]{:S(2)}, u32[]{:S(2)}) collective-permute-start(f32[2,512]{1,0:T(2,128)} %get-tuple-element.60), channel_id=1, source_target_pairs={{0,1},{1,0},{2,3},{3,2},{4,5},{5,4},{6,7},{7,6},{8,9},{9,8},{10,11... | collective-permute-start | bytes 12296 | tf_op jit(solution)/shard_map/ppermute | solution.py:21
  22.6 5.0 %collective-permute-start.3 = (bf16[8,512,128]{2,1,0:T(8,128)(2,1)}, bf16[8,512,128]{2,1,0:T(8,128)(2,1)S(1)}, u32[]{:S(2)}, u32[]{:S(2)}) collective-permute-start(bf16[8,512,128]{2,1,0:T(8,128)(2,1)} %get-tuple-element.69), channel_id=1, source_target_pairs={{0,2},{2,0},{4,6},{6,4},{8,10},{10,8},{12,14},{14,12},{16,18},{18,... | collective-permute-start | bytes 3145736 | tf_op jit(solution)/shard_map/ppermute | solution.py:21
  27.6 7.8 %copy-start.10 = (f32[2,512]{1,0:T(2,128)S(1)}, f32[2,512]{1,0:T(2,128)}, u32[]{:S(2)}) copy-start(f32[2,512]{1,0:T(2,128)} %get-tuple-element.67) | copy-start | bytes 12292
  27.6 1.0 %copy-start.1 = (bf16[8,512,128]{2,1,0:T(8,128)(2,1)}, bf16[8,512,128]{2,1,0:T(8,128)(2,1)S(1)}, u32[]{:S(2)}) copy-start(bf16[8,512,128]{2,1,0:T(8,128)(2,1)S(1)} %collective-permute-done.3.got_ref) | copy-start | bytes 3145732
  32.4 16.1 %collective-permute-start.4 = (bf16[4,256,128]{2,1,0:T(8,128)(2,1)}, bf16[4,256,128]{2,1,0:T(8,128)(2,1)}, u32[]{:S(2)}, u32[]{:S(2)}) collective-permute-start(bf16[4,256,128]{2,1,0:T(8,128)(2,1)} %get-tuple-element.73), channel_id=1, source_target_pairs={{0,4},{2,6},{4,0},{6,2},{8,12},{10,14},{12,8},{14,10},{16,20},{18,... | collective-permute-start | bytes 786440 | tf_op jit(solution)/shard_map/ppermute | solution.py:21
  33.9 14.6 %collective-permute-start.5 = (bf16[4,256,128]{2,1,0:T(8,128)(2,1)}, bf16[4,256,128]{2,1,0:T(8,128)(2,1)S(1)}, u32[]{:S(2)}, u32[]{:S(2)}) collective-permute-start(bf16[4,256,128]{2,1,0:T(8,128)(2,1)} %get-tuple-element.75), channel_id=1, source_target_pairs={{0,8},{2,10},{4,12},{6,14},{8,0},{10,2},{12,4},{14,6},{16,24},{18,... | collective-permute-start | bytes 786440 | tf_op jit(solution)/shard_map/ppermute | solution.py:21
  35.4 3.6 %collective-permute-start.2 = (f32[2,512]{1,0:T(2,128)S(1)}, f32[2,512]{1,0:T(2,128)S(1)}, u32[]{:S(2)}, u32[]{:S(2)}) collective-permute-start(f32[2,512]{1,0:T(2,128)S(1)} %copy-done.10), channel_id=1, source_target_pairs={{0,1},{1,0},{2,3},{3,2},{4,5},{5,4},{6,7},{7,6},{8,9},{9,8},{10,11... | collective-permute-start | bytes 12296 | tf_op jit(solution)/shard_map/ppermute | solution.py:21
  39.6 8.8 %copy-start.3 = (f32[4,256,128]{2,1,0:T(8,128)S(1)}, f32[4,256,128]{2,1,0:T(8,128)}, u32[]{:S(2)}) copy-start(f32[4,256,128]{2,1,0:T(8,128)} %get-tuple-element.82) | copy-start | bytes 1572868
  42.6 7.5 %copy-start.2 = (f32[4,256,128]{2,1,0:T(8,128)S(1)}, f32[4,256,128]{2,1,0:T(8,128)}, u32[]{:S(2)}) copy-start(f32[4,256,128]{2,1,0:T(8,128)} %get-tuple-element.84) | copy-start | bytes 1572868
  48.5 2.3 %copy-start.4 = (f32[40,512]{1,0:T(8,128)S(1)}, f32[40,512]{1,0:T(8,128)}, u32[]{:S(2)}) copy-start(f32[40,512]{1,0:T(8,128)} %shard_map.123) | copy-start | bytes 245764
  49.6 6.5 %collective-permute-start.6 = (bf16[2,256,128]{2,1,0:T(8,128)(2,1)S(1)}, bf16[2,256,128]{2,1,0:T(8,128)(2,1)S(1)}, u32[]{:S(2)}, u32[]{:S(2)}) collective-permute-start(bf16[2,256,128]{2,1,0:T(8,128)(2,1)S(1)} %slice.79), channel_id=1, source_target_pairs={{0,8},{2,10},{4,12},{6,14},{8,0},{10,2},{12,4},{14,6},{16,24},{18,... | collective-permute-start | bytes 393224 | tf_op jit(solution)/shard_map/ppermute | solution.py:21
  50.2 5.9 %collective-permute-start.7 = (bf16[2,256,128]{2,1,0:T(8,128)(2,1)S(1)}, bf16[2,256,128]{2,1,0:T(8,128)(2,1)S(1)}, u32[]{:S(2)}, u32[]{:S(2)}) collective-permute-start(bf16[2,256,128]{2,1,0:T(8,128)(2,1)S(1)} %slice.78), channel_id=1, source_target_pairs={{0,4},{2,6},{4,0},{6,2},{8,12},{10,14},{12,8},{14,10},{16,20},{18,... | collective-permute-start | bytes 393224 | tf_op jit(solution)/shard_map/ppermute | solution.py:21
  50.7 5.3 %collective-permute-start.8 = (f32[40,512]{1,0:T(8,128)S(1)}, f32[40,512]{1,0:T(8,128)}, u32[]{:S(2)}, u32[]{:S(2)}) collective-permute-start(f32[40,512]{1,0:T(8,128)S(1)} %copy-done.4), channel_id=1, source_target_pairs={{0,2},{2,0},{4,6},{6,4},{8,10},{10,8},{12,14},{14,12},{16,18},{18,... | collective-permute-start | bytes 245768 | tf_op jit(solution)/shard_map/ppermute | solution.py:21
  50.7 12.5 %collective-permute-start.11 = (f32[4,32,128]{2,1,0:T(8,128)}, f32[4,32,128]{2,1,0:T(8,128)S(1)}, u32[]{:S(2)}, u32[]{:S(2)}) collective-permute-start(f32[4,32,128]{2,1,0:T(8,128)} %get-tuple-element.98), channel_id=1, source_target_pairs={{2,0},{4,2},{6,4},{8,6},{10,8},{12,10},{14,12},{16,14},{18,16},{20... | collective-permute-start | bytes 196616 | tf_op jit(solution)/shard_map/ppermute | solution.py:16
  56.8 11.1 %collective-permute-start.9 = (bf16[1,512,128]{2,1,0:T(8,128)(2,1)}, bf16[1,512,128]{2,1,0:T(8,128)(2,1)}, u32[]{:S(2)}, u32[]{:S(2)}) collective-permute-start(bf16[1,512,128]{2,1,0:T(8,128)(2,1)} %fusion.5), channel_id=1, source_target_pairs={{0,16},{2,18},{4,20},{6,22},{8,24},{10,26},{12,28},{14,30},{16,0},... | collective-permute-start | bytes 393224 | tf_op jit(solution)/shard_map/ppermute | solution.py:21
  62.4 12.6 %copy-start.5 = (bf16[256,512]{1,0:T(8,128)(2,1)S(1)}, bf16[256,512]{1,0:T(8,128)(2,1)}, u32[]{:S(2)}) copy-start(bf16[256,512]{1,0:T(8,128)(2,1)} %get-tuple-element.90) | copy-start | bytes 786436
  62.4 12.5 %copy-start.6 = (bf16[256,512]{1,0:T(8,128)(2,1)S(1)}, bf16[256,512]{1,0:T(8,128)(2,1)}, u32[]{:S(2)}) copy-start(bf16[256,512]{1,0:T(8,128)(2,1)} %get-tuple-element.102) | copy-start | bytes 786436
  62.4 5.5 %collective-permute-start.10 = (f32[40,512]{1,0:T(8,128)S(1)}, f32[40,512]{1,0:T(8,128)}, u32[]{:S(2)}, u32[]{:S(2)}) collective-permute-start(f32[40,512]{1,0:T(8,128)S(1)} %add.43), channel_id=1, source_target_pairs={{0,4},{2,6},{4,0},{6,2},{8,12},{10,14},{12,8},{14,10},{16,20},{18,... | collective-permute-start | bytes 245768 | tf_op jit(solution)/shard_map/ppermute | solution.py:21
  63.2 0.6 copy-start.8
  67.9 7.1 %copy-start.7 = (bf16[256,512]{1,0:T(8,128)(2,1)S(1)}, bf16[256,512]{1,0:T(8,128)(2,1)}, u32[]{:S(2)}) copy-start(bf16[256,512]{1,0:T(8,128)(2,1)} %get-tuple-element.101) | copy-start | bytes 786436
  68.9 4.5 %collective-permute-start.12 = (f32[40,512]{1,0:T(8,128)S(1)}, f32[40,512]{1,0:T(8,128)S(1)}, u32[]{:S(2)}, u32[]{:S(2)}) collective-permute-start(f32[40,512]{1,0:T(8,128)S(1)} %add.44), channel_id=1, source_target_pairs={{0,8},{2,10},{4,12},{6,14},{8,0},{10,2},{12,4},{14,6},{16,24},{18,... | collective-permute-start | bytes 245768 | tf_op jit(solution)/shard_map/ppermute | solution.py:21
  73.4 5.4 %collective-permute-start.13 = (f32[40,512]{1,0:T(8,128)S(1)}, f32[40,512]{1,0:T(8,128)S(1)}, u32[]{:S(2)}, u32[]{:S(2)}) collective-permute-start(f32[40,512]{1,0:T(8,128)S(1)} %add.45), channel_id=1, source_target_pairs={{0,16},{2,18},{4,20},{6,22},{8,24},{10,26},{12,28},{14,30},{16,0},... | collective-permute-start | bytes 245768 | tf_op jit(solution)/shard_map/ppermute | solution.py:21

commit v3 on v2

--- a/solution.py
+++ b/solution.py
@@ -41,13 +41,15 @@
 
 def call(body, outs, *args, scalars=0, scratch=()):
     vmem = pl.BlockSpec(memory_space=pltpu.VMEM)
+    resident = [pltpu.with_memory_space_constraint(a, pltpu.VMEM) for a in args[scalars:]]
     return pl.pallas_call(
         body,
         in_specs=[pl.BlockSpec(memory_space=pltpu.SMEM)] * scalars + [vmem] * (len(args) - scalars),
         out_specs=[vmem] * len(outs),
-        out_shape=[jax.ShapeDtypeStruct(shape, kind) for shape, kind in outs],
+        out_shape=[pltpu.VMEM(shape, kind) for shape, kind in outs],
         scratch_shapes=list(scratch),
-    )(*args)
+        compiler_params=pltpu.CompilerParams(vmem_limit_bytes=20 * 1024 * 1024),
+    )(*args[:scalars], *resident)
 
 
 def group(g):
@@ -268,7 +270,7 @@
     return call(body, [((height, groups * LANES), jnp.float32)], grad_conv, padded, columns)[0]
 
 
-def conv_backward(grad_conv, ahead, conv_taps, value, gate, start):
+def conv_backward(grad_conv, ahead, conv_taps, value, gate, start, top=None):
     groups, rows, _ = grad_conv.shape
     taps = conv_taps.shape[0]
     count = rows // 2
@@ -277,7 +279,10 @@
 
     def body(*refs):
         if final:
-            grad_ref, ahead_ref, taps_ref, value_ref, gate_ref, gv_ref, gg_ref, held_ref = refs
+            grad_ref, ahead_ref, taps_ref, value_ref, gate_ref, tv_ref, tg_ref = refs[:7]
+            gv_ref, gg_ref, held_ref = refs[7:]
+            gv_ref[:start] = tv_ref[...]
+            gg_ref[:start] = tg_ref[...]
             held_ref[:, :count, :] = grad_ref[:, start:, :]
             held_ref[:, count:, :] = ahead_ref[...]
             source, base = held_ref, 0
@@ -297,8 +302,8 @@
                 here = pl.ds(first + start, TILE)
                 v = value_ref[here, group(g)].astype(jnp.float32)
                 s = jax.nn.sigmoid(gate_ref[here, group(g)].astype(jnp.float32))
-                gv_ref[pl.ds(first, TILE), group(g)] = (total * s).astype(jnp.bfloat16)
-                gg_ref[pl.ds(first, TILE), group(g)] = (total * v * s * (1.0 - s)).astype(jnp.bfloat16)
+                gv_ref[here, group(g)] = (total * s).astype(jnp.bfloat16)
+                gg_ref[here, group(g)] = (total * v * s * (1.0 - s)).astype(jnp.bfloat16)
                 return carry
 
             lax.fori_loop(0, count // TILE, tile, 0)
@@ -306,7 +311,8 @@
     outs = [((count, width), jnp.bfloat16)] * 2
     if final:
         scratch = [pltpu.VMEM((groups, count + ahead.shape[1], LANES), jnp.float32)]
-        return call(body, outs, grad_conv, ahead, conv_taps, value, gate, scratch=scratch)
+        outs = [((rows, width), jnp.bfloat16)] * 2
+        return call(body, outs, grad_conv, ahead, conv_taps, value, gate, *top, scratch=scratch)
     return call(body, outs, grad_conv, conv_taps, value, gate)
 
 
@@ -399,7 +405,7 @@
         both = halved(both, "sp", 3)
         summed = summed[0] + summed[1]
         summed = (summed, swapped(summed, "sp", 1))
-    bottom = conv_backward(grad_conv, ahead, conv_taps, glu_value, glu_gate, cut)
+    bottom = conv_backward(grad_conv, ahead, conv_taps, glu_value, glu_gate, cut, top)
     if by_halves:
         both, summed, bottom = together(both, summed, bottom)
         grad_proj = added(both)[0].T
@@ -408,9 +414,7 @@
             summed = summed + swapped(summed, "sp", bit)
     else:
         summed = summed_over(summed, "sp")
-    grad_value = jnp.concatenate([top[0], bottom[0]], axis=0)
-    grad_gate = jnp.concatenate([top[1], bottom[1]], axis=0)
-    return (grad_value, grad_gate, summed[:taps], summed[taps], summed[taps + 1], grad_proj)
+    return (bottom[0], bottom[1], summed[:taps], summed[taps], summed[taps + 1], grad_proj)
 
 
 def solution(mesh):

time: 80.6 us -> 58.6 us (0.73)
  Pallas kernels: 33.6 us -> 13.4 us
  other arithmetic: 8.74 us -> 1.26 us
  waiting for transfers between devices: 6.03 us -> 13.3 us
  matrix products: 5.54 us -> 4.72 us
    pallas_call x8, Pallas kernels: 33.6 us -> 13.4 us  [call(): pl.pallas_call(body, in_specs=[pl.BlockSpec(memory_space=pltpu.SMEM)] * s...]
    ppermute x12, waiting for transfers between devices: 6.03 us -> 13.3 us  [swapped(): return lax.ppermute(shard, axis, [(i, i ^ 1 << bit) for i in range(size)])]
    concatenate x1 -> x0, other arithmetic: 1.98 us -> none  [on_device(): grad_value = jnp.concatenate([top[0], bottom[0]], axis=0)]
    add x2, other arithmetic: 1.83 us -> 0.03 us  [on_device(): summed = summed[0] + summed[1]]
    add x2, other arithmetic: 1.18 us -> 0.01 us  [summed_over(): shard = shard + swapped(shard, axis, bit)]
    add x4 -> x3, other arithmetic: 1.12 us -> 0.18 us  [added(): return pair[0] + pair[1].astype(jnp.float32)]
    transpose x1, other arithmetic: 0.94 us -> 0.03 us  [on_device(): grad_proj = added(both)[0].T]
    dot_general x2, matrix products: 5.54 us -> 4.72 us  [act_gradient(): lax.dot_general(part, out_proj, (((1,), (1,)), ((), ())), preferred_eleme...]
  transfers between devices with their start and end apart: 14 -> 14, of which waited for: 3 -> 8; matrix products, arithmetic and copies ran while one was open for 15% -> 13% of each run, Pallas kernels for 25% -> 14%
where the time goes in v3:
time: 58.6 us; the launch traced here: 58.4 us
  starting transfers between devices  21 us (36%)
  Pallas kernels  13.4 us (23%)
  waiting for transfers between devices  13.3 us (23%)
  matrix products  4.72 us (8%)
  local copies, waits for them, and re-layouts  3.78 us (6%)
  other arithmetic  1.26 us (2%)
  between operations  0.93 us (2%)
    ppermute x12, starting transfers between devices, swapped(): return lax.ppermute(shard, axis, [(i, i ^ 1 << bit) for i in range(size)])  17.3 us
    pallas_call x8, Pallas kernels, call(): pl.pallas_call(body, in_specs=[pl.BlockSpec(memory_space=pltpu.SMEM)] * s...  13.4 us
    ppermute x12, waiting for transfers between devices, swapped(): return lax.ppermute(shard, axis, [(i, i ^ 1 << bit) for i in range(size)])  13.3 us
    dot_general x2, matrix products, act_gradient(): lax.dot_general(part, out_proj, (((1,), (1,)), ((), ())), preferred_eleme...  4.72 us
    ppermute x2, starting transfers between devices, passed_along(): return lax.ppermute(shard, axis, pairs)  3.68 us
    unnamed x21, local copies, waits for them, and re-layouts  2.48 us
  transfers between devices with their start and end apart: 14, of which 8 were waited for; matrix products, arithmetic and copies ran while one was open for 13% of the time, Pallas kernels for 14%

profile of v3, /device:TPU:0, one launch (start us, length us, event | category | flops | bytes accessed | tf_op | source)
XLA Modules:
  0.0 58.4 jit_solution(9958888564080579464)
XLA Ops:
  0.6 0.0 copy-start
  0.6 0.0 copy-start.3
  0.7 0.0 copy-start.2
  0.7 0.0 copy-start.5
  0.7 1.0 %multiply_convert_fusion = bf16[32,512]{1,0:T(8,128)(2,1)S(1)} fusion(bf16[512,512]{1,0:T(8,128)(2,1)} %refs_4_.1, bf16[512,512]{1,0:T(8,128)(2,1)} %refs_3_.3), kind=kLoop, calls=%fused_computation.16 | loop fusion | flops 114688 | bytes 98304 | tf_op jit(solution)/shard_map/convert_element_type | solution.py:352
  1.6 2.4 %collective-permute-start = (bf16[32,512]{1,0:T(8,128)(2,1)S(1)}, bf16[32,512]{1,0:T(8,128)(2,1)S(1)}, u32[]{:S(2)}, u32[]{:S(2)}) collective-permute-start(bf16[32,512]{1,0:T(8,128)(2,1)S(1)} %multiply_convert_fusion), channel_id=1, source_target_pairs={{0,2},{2,4},{4,6},{6,8},{8,10},{10,12},{12,14},{14,16},{16,18},{18... | collective-permute-start | bytes 98312 | tf_op jit(solution)/shard_map/ppermute | solution.py:16
  4.0 0.0 copy-done
  4.1 2.8 %fusion.2.up_ref = f32[256,512]{1,0:T(8,128)} fusion(bf16[512,2048]{1,0:T(8,128)(2,1)S(1)} %copy-done, bf16[512,2048]{1,0:T(8,128)(2,1)} %grad_ref.3), kind=kOutput, calls=%fused_computation.2 | convolution fusion | flops 536870912 | bytes 3670016 | tf_op jit(solution)/shard_map/dot_general | solution.py:356
  6.8 0.0 collective-permute-done.before_ref
  6.8 0.0 copy-done.3
  6.8 0.0 copy-done.2
  6.8 0.0 copy-done.5
  6.8 3.2 %shard_map.118 = (f32[512,512]{1,0:T(8,128)S(1)}, f32[4,544,128]{2,1,0:T(8,128)S(1)}, f32[2,512]{1,0:T(2,128)S(1)}) custom-call(bf16[512,512]{1,0:T(8,128)(2,1)S(1)} %copy-done.2, bf16[512,512]{1,0:T(8,128)(2,1)S(1)} %copy-done.3, bf16[32,512]{1,0:T(8,128)(2,1)S(1)} %collective-permute-done.before_ref, f32[31,512]{1,0:T(8,128)S(1)} %copy-done.5), custom_call_target="tpu_custom_call" | custom-call | tf_op jit(solution)/shard_map/pallas_call | solution.py:45
  10.1 0.0 copy-start.1
  10.1 0.0 copy-start.7
  10.1 0.0 copy-start.8
  10.1 2.4 %collective-permute-start.1 = (f32[2,512]{1,0:T(2,128)S(1)}, f32[2,512]{1,0:T(2,128)S(1)}, u32[]{:S(2)}, u32[]{:S(2)}) collective-permute-start(f32[2,512]{1,0:T(2,128)S(1)} %get-tuple-element.60), channel_id=1, source_target_pairs={{0,1},{1,0},{2,3},{3,2},{4,5},{5,4},{6,7},{7,6},{8,9},{9,8},{10,11... | collective-permute-start | bytes 12296 | tf_op jit(solution)/shard_map/ppermute | solution.py:21
  12.5 2.0 %fusion.low_ref = f32[256,512]{1,0:T(8,128)S(1)} fusion(bf16[512,2048]{1,0:T(8,128)(2,1)S(1)} %copy-done, bf16[512,2048]{1,0:T(8,128)(2,1)} %grad_ref.3), kind=kOutput, calls=%fused_computation | convolution fusion | flops 536870912 | bytes 3670016 | tf_op jit(solution)/shard_map/dot_general | solution.py:356
  14.4 0.0 copy-start.6
  14.5 0.0 collective-permute-done.1
  14.5 0.0 copy-done.1
  14.5 0.0 copy-done.7
  14.5 0.0 copy-done.8
  14.5 1.1 %shard_map.119 = (bf16[512,512]{1,0:T(8,128)(2,1)S(1)}, bf16[8,512,128]{2,1,0:T(8,128)(2,1)S(1)}) custom-call(s32[1]{0:T(128)} %bitcast.me_ref, f32[512,512]{1,0:T(8,128)S(1)} %get-tuple-element.58.conv_ref, f32[2,512]{1,0:T(2,128)S(1)} %add.37.sums_ref, f32[1,512]{1,0:T(1,128)S(1)} %bitcast.11, f32[1,512]{1,0:T(1,128)S(1)} %bitcast.13, ...), custom_call_target="tpu_custom_call" | custom-call | tf_op jit(solution)/shard_map/pallas_call | solution.py:45
  15.6 1.6 %collective-permute-start.3 = (bf16[8,512,128]{2,1,0:T(8,128)(2,1)S(1)}, bf16[8,512,128]{2,1,0:T(8,128)(2,1)S(1)}, u32[]{:S(2)}, u32[]{:S(2)}) collective-permute-start(bf16[8,512,128]{2,1,0:T(8,128)(2,1)S(1)} %get-tuple-element.69), channel_id=1, source_target_pairs={{0,2},{2,0},{4,6},{6,4},{8,10},{10,8},{12,14},{14,12},{16,18},{18,... | collective-permute-start | bytes 3145736 | tf_op jit(solution)/shard_map/ppermute | solution.py:21
  17.2 0.0 copy-done.6
  17.2 0.9 %shard_map.120 = (f32[512,512]{1,0:T(8,128)S(1)}, f32[512,512]{1,0:T(8,128)S(1)}, f32[2,512]{1,0:T(2,128)S(1)}, f32[2,512]{1,0:T(2,128)S(1)}) custom-call(f32[512,512]{1,0:T(8,128)S(1)} %get-tuple-element.58.conv_ref, f32[2,512]{1,0:T(2,128)S(1)} %add.37.sums_ref, f32[1,512]{1,0:T(1,128)S(1)} %bitcast.12, f32[1,512]{1,0:T(1,128)S(1)} %bitcast.14, ...), custom_call_target="tpu_custom_call" | custom-call | tf_op jit(solution)/shard_map/pallas_call | solution.py:45
  18.1 1.4 %collective-permute-done.3.got_ref = bf16[8,512,128]{2,1,0:T(8,128)(2,1)S(1)} collective-permute-done((bf16[8,512,128]{2,1,0:T(8,128)(2,1)S(1)}, bf16[8,512,128]{2,1,0:T(8,128)(2,1)S(1)}, u32[]{:S(2)}, u32[]{:S(2)}) %collective-permute-start.3) | collective-permute-done | bytes 1048608 | tf_op jit(solution)/shard_map/ppermute | solution.py:21
  19.5 0.8 %shard_map.121 = (f32[4,256,128]{2,1,0:T(8,128)S(1)}, bf16[4,256,128]{2,1,0:T(8,128)(2,1)S(1)}, f32[4,256,128]{2,1,0:T(8,128)S(1)}, bf16[4,256,128]{2,1,0:T(8,128)(2,1)S(1)}) custom-call(s32[1]{0:T(128)} %bitcast.me_ref, bf16[512,512]{1,0:T(8,128)(2,1)S(1)} %get-tuple-element.68.act_ref, bf16[512,2048]{1,0:T(8,128)(2,1)S(1)} %copy-done.1, ...), custom_call_target="tpu_custom_call" | custom-call | tf_op jit(solution)/shard_map/pallas_call | solution.py:45
  20.3 1.6 %collective-permute-start.4 = (bf16[4,256,128]{2,1,0:T(8,128)(2,1)S(1)}, bf16[4,256,128]{2,1,0:T(8,128)(2,1)S(1)}, u32[]{:S(2)}, u32[]{:S(2)}) collective-permute-start(bf16[4,256,128]{2,1,0:T(8,128)(2,1)S(1)} %get-tuple-element.73), channel_id=1, source_target_pairs={{0,4},{2,6},{4,0},{6,2},{8,12},{10,14},{12,8},{14,10},{16,20},{18,... | collective-permute-start | bytes 786440 | tf_op jit(solution)/shard_map/ppermute | solution.py:21
  21.9 1.6 %collective-permute-start.5 = (bf16[4,256,128]{2,1,0:T(8,128)(2,1)S(1)}, bf16[4,256,128]{2,1,0:T(8,128)(2,1)S(1)}, u32[]{:S(2)}, u32[]{:S(2)}) collective-permute-start(bf16[4,256,128]{2,1,0:T(8,128)(2,1)S(1)} %get-tuple-element.75), channel_id=1, source_target_pairs={{0,8},{2,10},{4,12},{6,14},{8,0},{10,2},{12,4},{14,6},{16,24},{18,... | collective-permute-start | bytes 786440 | tf_op jit(solution)/shard_map/ppermute | solution.py:21
  23.5 1.1 %collective-permute-start.2 = (f32[2,512]{1,0:T(2,128)S(1)}, f32[2,512]{1,0:T(2,128)S(1)}, u32[]{:S(2)}, u32[]{:S(2)}) collective-permute-start(f32[2,512]{1,0:T(2,128)S(1)} %get-tuple-element.67), channel_id=1, source_target_pairs={{0,1},{1,0},{2,3},{3,2},{4,5},{5,4},{6,7},{7,6},{8,9},{9,8},{10,11... | collective-permute-start | bytes 12296 | tf_op jit(solution)/shard_map/ppermute | solution.py:21
  24.6 2.5 %collective-permute-done.2 = f32[2,512]{1,0:T(2,128)S(1)} collective-permute-done((f32[2,512]{1,0:T(2,128)S(1)}, f32[2,512]{1,0:T(2,128)S(1)}, u32[]{:S(2)}, u32[]{:S(2)}) %collective-permute-start.2) | collective-permute-done | bytes 4128 | tf_op jit(solution)/shard_map/ppermute | solution.py:21
  27.1 0.4 shard_map.122
  27.5 3.6 %shard_map.123 = f32[40,512]{1,0:T(8,128)S(1)} custom-call(f32[4,512,128]{2,1,0:T(8,128)S(1)} %get-tuple-element.96.grad_ref.refs_0_, f32[4,544,128]{2,1,0:T(8,128)S(1)} %get-tuple-element.80.padded_ref, f32[2,512]{1,0:T(2,128)S(1)} %get-tuple-element.81.col_ref), custom_call_target="tpu_custom_call" | custom-call | tf_op jit(solution)/shard_map/pallas_call | solution.py:45
  31.1 0.0 collective-permute-done.4
  31.1 0.0 collective-permute-done.5
  31.1 0.1 convert_add_fusion.1
  31.2 0.7 %collective-permute-start.6 = (bf16[2,256,128]{2,1,0:T(8,128)(2,1)S(1)}, bf16[2,256,128]{2,1,0:T(8,128)(2,1)S(1)}, u32[]{:S(2)}, u32[]{:S(2)}) collective-permute-start(bf16[2,256,128]{2,1,0:T(8,128)(2,1)S(1)} %slice.79), channel_id=1, source_target_pairs={{0,8},{2,10},{4,12},{6,14},{8,0},{10,2},{12,4},{14,6},{16,24},{18,... | collective-permute-start | bytes 393224 | tf_op jit(solution)/shard_map/ppermute | solution.py:21
  31.9 0.1 convert_add_fusion
  32.0 0.9 %collective-permute-start.7 = (bf16[2,256,128]{2,1,0:T(8,128)(2,1)S(1)}, bf16[2,256,128]{2,1,0:T(8,128)(2,1)S(1)}, u32[]{:S(2)}, u32[]{:S(2)}) collective-permute-start(bf16[2,256,128]{2,1,0:T(8,128)(2,1)S(1)} %slice.78), channel_id=1, source_target_pairs={{0,4},{2,6},{4,0},{6,2},{8,12},{10,14},{12,8},{14,10},{16,20},{18,... | collective-permute-start | bytes 393224 | tf_op jit(solution)/shard_map/ppermute | solution.py:21
  32.9 0.0 collective-permute-start.8
  32.9 1.3 %collective-permute-start.11 = (f32[4,32,128]{2,1,0:T(8,128)S(1)}, f32[4,32,128]{2,1,0:T(8,128)S(1)}, u32[]{:S(2)}, u32[]{:S(2)}) collective-permute-start(f32[4,32,128]{2,1,0:T(8,128)S(1)} %get-tuple-element.97), channel_id=1, source_target_pairs={{2,0},{4,2},{6,4},{8,6},{10,8},{12,10},{14,12},{16,14},{18,16},{20... | collective-permute-start | bytes 196616 | tf_op jit(solution)/shard_map/ppermute | solution.py:16
  34.2 0.0 copy-start.4
  34.2 1.7 %shard_map.124 = (bf16[256,512]{1,0:T(8,128)(2,1)S(1)}, bf16[256,512]{1,0:T(8,128)(2,1)S(1)}) custom-call(f32[4,512,128]{2,1,0:T(8,128)S(1)} %get-tuple-element.96.grad_ref.refs_0_, f32[31,512]{1,0:T(8,128)S(1)} %copy-done.5, bf16[512,512]{1,0:T(8,128)(2,1)S(1)} %copy-done.2, bf16[512,512]{1,0:T(8,128)(2,1)S(1)} %copy-done.3), custom_call_target="tpu_custom_call" | custom-call | tf_op jit(solution)/shard_map/pallas_call | solution.py:45
  35.9 0.0 collective-permute-done.8
  35.9 0.3 collective-permute-done.6
  36.2 0.8 %collective-permute-done.7 = bf16[2,256,128]{2,1,0:T(8,128)(2,1)S(1)} collective-permute-done((bf16[2,256,128]{2,1,0:T(8,128)(2,1)S(1)}, bf16[2,256,128]{2,1,0:T(8,128)(2,1)S(1)}, u32[]{:S(2)}, u32[]{:S(2)}) %collective-permute-start.7) | collective-permute-done | bytes 131104 | tf_op jit(solution)/shard_map/ppermute | solution.py:21
  37.1 0.1 convert_add_fusion.2
  37.1 3.2 %collective-permute-start.9 = (bf16[1,512,128]{2,1,0:T(8,128)(2,1)S(1)}, bf16[1,512,128]{2,1,0:T(8,128)(2,1)S(1)}, u32[]{:S(2)}, u32[]{:S(2)}) collective-permute-start(bf16[1,512,128]{2,1,0:T(8,128)(2,1)S(1)} %fusion.5), channel_id=1, source_target_pairs={{0,16},{2,18},{4,20},{6,22},{8,24},{10,26},{12,28},{14,30},{16,0},... | collective-permute-start | bytes 393224 | tf_op jit(solution)/shard_map/ppermute | solution.py:21
  40.3 1.2 %collective-permute-start.10 = (f32[40,512]{1,0:T(8,128)S(1)}, f32[40,512]{1,0:T(8,128)S(1)}, u32[]{:S(2)}, u32[]{:S(2)}) collective-permute-start(f32[40,512]{1,0:T(8,128)S(1)} %add.43), channel_id=1, source_target_pairs={{0,4},{2,6},{4,0},{6,2},{8,12},{10,14},{12,8},{14,10},{16,20},{18,... | collective-permute-start | bytes 245768 | tf_op jit(solution)/shard_map/ppermute | solution.py:21
  41.5 0.0 collective-permute-done.11.refs_1_
  41.5 1.7 %shard_map.125 = (bf16[512,512]{1,0:T(8,128)(2,1)S(1)}, bf16[512,512]{1,0:T(8,128)(2,1)S(1)}) custom-call(f32[4,512,128]{2,1,0:T(8,128)S(1)} %get-tuple-element.96.grad_ref.refs_0_, f32[4,32,128]{2,1,0:T(8,128)S(1)} %collective-permute-done.11.refs_1_, f32[31,512]{1,0:T(8,128)S(1)} %copy-done.5, bf16[512,512]{1,0:T(8,128)(2,1)S(1)} %copy-done.2, ...), custom_call_target="tpu_custom_call" | custom-call | tf_op jit(solution)/shard_map/pallas_call | solution.py:45
  43.3 1.5 %collective-permute-done.10 = f32[40,512]{1,0:T(8,128)S(1)} collective-permute-done((f32[40,512]{1,0:T(8,128)S(1)}, f32[40,512]{1,0:T(8,128)S(1)}, u32[]{:S(2)}, u32[]{:S(2)}) %collective-permute-start.10) | collective-permute-done | bytes 81952 | tf_op jit(solution)/shard_map/ppermute | solution.py:21
  44.8 1.5 %collective-permute-done.9 = bf16[1,512,128]{2,1,0:T(8,128)(2,1)S(1)} collective-permute-done((bf16[1,512,128]{2,1,0:T(8,128)(2,1)S(1)}, bf16[1,512,128]{2,1,0:T(8,128)(2,1)S(1)}, u32[]{:S(2)}, u32[]{:S(2)}) %collective-permute-start.9) | collective-permute-done | bytes 131104 | tf_op jit(solution)/shard_map/ppermute | solution.py:21
  46.3 0.8 %collective-permute-start.12 = (f32[40,512]{1,0:T(8,128)S(1)}, f32[40,512]{1,0:T(8,128)S(1)}, u32[]{:S(2)}, u32[]{:S(2)}) collective-permute-start(f32[40,512]{1,0:T(8,128)S(1)} %add.44), channel_id=1, source_target_pairs={{0,8},{2,10},{4,12},{6,14},{8,0},{10,2},{12,4},{14,6},{16,24},{18,... | collective-permute-start | bytes 245768 | tf_op jit(solution)/shard_map/ppermute | solution.py:21
  47.1 3.7 %collective-permute-done.12 = f32[40,512]{1,0:T(8,128)S(1)} collective-permute-done((f32[40,512]{1,0:T(8,128)S(1)}, f32[40,512]{1,0:T(8,128)S(1)}, u32[]{:S(2)}, u32[]{:S(2)}) %collective-permute-start.12) | collective-permute-done | bytes 81952 | tf_op jit(solution)/shard_map/ppermute | solution.py:21
  50.9 2.3 %collective-permute-start.13 = (f32[40,512]{1,0:T(8,128)S(1)}, f32[40,512]{1,0:T(8,128)S(1)}, u32[]{:S(2)}, u32[]{:S(2)}) collective-permute-start(f32[40,512]{1,0:T(8,128)S(1)} %add.45), channel_id=1, source_target_pairs={{0,16},{2,18},{4,20},{6,22},{8,24},{10,26},{12,28},{14,30},{16,0},... | collective-permute-start | bytes 245768 | tf_op jit(solution)/shard_map/ppermute | solution.py:21
  53.2 0.8 %copy.14 = bf16[512,512]{1,0:T(8,128)(2,1)} copy(bf16[512,512]{1,0:T(8,128)(2,1)S(1)} %get-tuple-element.118) | data formatting | bytes 1048576
  54.0 0.8 %copy.13 = f32[128,512]{1,0:T(8,128)} copy(f32[128,512]{0,1:T(8,128)S(1)} %add_bitcast_fusion) | data formatting | bytes 524288
  54.9 0.8 %copy.15 = bf16[512,512]{1,0:T(8,128)(2,1)} copy(bf16[512,512]{1,0:T(8,128)(2,1)S(1)} %get-tuple-element.119) | data formatting | bytes 1048576
  55.7 1.5 %collective-permute-done.13 = f32[40,512]{1,0:T(8,128)S(1)} collective-permute-done((f32[40,512]{1,0:T(8,128)S(1)}, f32[40,512]{1,0:T(8,128)S(1)}, u32[]{:S(2)}, u32[]{:S(2)}) %collective-permute-start.13) | collective-permute-done | bytes 81952 | tf_op jit(solution)/shard_map/ppermute | solution.py:21
  57.2 0.6 %fusion.6 = (f32[1,512]{1,0:T(1,128)}, f32[1,512]{1,0:T(1,128)}) fusion(f32[40,512]{1,0:T(8,128)S(1)} %add.46), kind=kLoop, calls=%fused_computation.17 | loop fusion | bytes 8192 | tf_op jit(solution)/shard_map/slice | solution.py:417
  57.8 0.6 %slice.61 = f32[31,512]{1,0:T(8,128)} slice(f32[40,512]{1,0:T(8,128)S(1)} %add.46), slice={[0:31], [0:512]} | slice | bytes 126976 | tf_op jit(solution)/shard_map/slice | solution.py:417
  (14 shorter events, 0.2 us)
Async XLA Ops:
  0.6 3.4 %copy-start = (bf16[512,2048]{1,0:T(8,128)(2,1)S(1)}, bf16[512,2048]{1,0:T(8,128)(2,1)}, u32[]{:S(2)}) copy-start(bf16[512,2048]{1,0:T(8,128)(2,1)} %param.12) | copy-start | bytes 6291460
  0.6 6.2 %copy-start.3 = (bf16[512,512]{1,0:T(8,128)(2,1)S(1)}, bf16[512,512]{1,0:T(8,128)(2,1)}, u32[]{:S(2)}) copy-start(bf16[512,512]{1,0:T(8,128)(2,1)} %refs_4_.1) | copy-start | bytes 1572868
  0.7 6.2 %copy-start.2 = (bf16[512,512]{1,0:T(8,128)(2,1)S(1)}, bf16[512,512]{1,0:T(8,128)(2,1)}, u32[]{:S(2)}) copy-start(bf16[512,512]{1,0:T(8,128)(2,1)} %refs_3_.3) | copy-start | bytes 1572868
  0.7 6.2 %copy-start.5 = (f32[31,512]{1,0:T(8,128)S(1)}, f32[31,512]{1,0:T(8,128)}, u32[]{:S(2)}) copy-start(f32[31,512]{1,0:T(8,128)} %refs_2_.3) | copy-start | bytes 190468
  1.6 5.2 %collective-permute-start = (bf16[32,512]{1,0:T(8,128)(2,1)S(1)}, bf16[32,512]{1,0:T(8,128)(2,1)S(1)}, u32[]{:S(2)}, u32[]{:S(2)}) collective-permute-start(bf16[32,512]{1,0:T(8,128)(2,1)S(1)} %multiply_convert_fusion), channel_id=1, source_target_pairs={{0,2},{2,4},{4,6},{6,8},{8,10},{10,12},{12,14},{14,16},{16,18},{18... | collective-permute-start | bytes 98312 | tf_op jit(solution)/shard_map/ppermute | solution.py:16
  10.1 4.4 %copy-start.1 = (bf16[512,2048]{1,0:T(8,128)(2,1)S(1)}, bf16[512,2048]{1,0:T(8,128)(2,1)}, u32[]{:S(2)}) copy-start(bf16[512,2048]{1,0:T(8,128)(2,1)} %grad_ref.3) | copy-start | bytes 6291460
  10.1 4.4 %copy-start.7 = (f32[512]{0:T(512)S(1)}, f32[512]{0:T(512)}, u32[]{:S(2)}) copy-start(f32[512]{0:T(512)} %param.10) | copy-start | bytes 6148
  10.1 4.4 %copy-start.8 = (f32[512]{0:T(512)S(1)}, f32[512]{0:T(512)}, u32[]{:S(2)}) copy-start(f32[512]{0:T(512)} %param.11) | copy-start | bytes 6148
  10.1 4.4 %collective-permute-start.1 = (f32[2,512]{1,0:T(2,128)S(1)}, f32[2,512]{1,0:T(2,128)S(1)}, u32[]{:S(2)}, u32[]{:S(2)}) collective-permute-start(f32[2,512]{1,0:T(2,128)S(1)} %get-tuple-element.60), channel_id=1, source_target_pairs={{0,1},{1,0},{2,3},{3,2},{4,5},{5,4},{6,7},{7,6},{8,9},{9,8},{10,11... | collective-permute-start | bytes 12296 | tf_op jit(solution)/shard_map/ppermute | solution.py:21
  14.4 2.8 %copy-start.6 = (f32[256,512]{1,0:T(8,128)S(1)}, f32[256,512]{1,0:T(8,128)}, u32[]{:S(2)}) copy-start(f32[256,512]{1,0:T(8,128)} %fusion.2.up_ref) | copy-start | bytes 1572868
  15.6 3.9 %collective-permute-start.3 = (bf16[8,512,128]{2,1,0:T(8,128)(2,1)S(1)}, bf16[8,512,128]{2,1,0:T(8,128)(2,1)S(1)}, u32[]{:S(2)}, u32[]{:S(2)}) collective-permute-start(bf16[8,512,128]{2,1,0:T(8,128)(2,1)S(1)} %get-tuple-element.69), channel_id=1, source_target_pairs={{0,2},{2,0},{4,6},{6,4},{8,10},{10,8},{12,14},{14,12},{16,18},{18,... | collective-permute-start | bytes 3145736 | tf_op jit(solution)/shard_map/ppermute | solution.py:21
  20.3 10.8 %collective-permute-start.4 = (bf16[4,256,128]{2,1,0:T(8,128)(2,1)S(1)}, bf16[4,256,128]{2,1,0:T(8,128)(2,1)S(1)}, u32[]{:S(2)}, u32[]{:S(2)}) collective-permute-start(bf16[4,256,128]{2,1,0:T(8,128)(2,1)S(1)} %get-tuple-element.73), channel_id=1, source_target_pairs={{0,4},{2,6},{4,0},{6,2},{8,12},{10,14},{12,8},{14,10},{16,20},{18,... | collective-permute-start | bytes 786440 | tf_op jit(solution)/shard_map/ppermute | solution.py:21
  21.9 9.2 %collective-permute-start.5 = (bf16[4,256,128]{2,1,0:T(8,128)(2,1)S(1)}, bf16[4,256,128]{2,1,0:T(8,128)(2,1)S(1)}, u32[]{:S(2)}, u32[]{:S(2)}) collective-permute-start(bf16[4,256,128]{2,1,0:T(8,128)(2,1)S(1)} %get-tuple-element.75), channel_id=1, source_target_pairs={{0,8},{2,10},{4,12},{6,14},{8,0},{10,2},{12,4},{14,6},{16,24},{18,... | collective-permute-start | bytes 786440 | tf_op jit(solution)/shard_map/ppermute | solution.py:21
  23.5 3.6 %collective-permute-start.2 = (f32[2,512]{1,0:T(2,128)S(1)}, f32[2,512]{1,0:T(2,128)S(1)}, u32[]{:S(2)}, u32[]{:S(2)}) collective-permute-start(f32[2,512]{1,0:T(2,128)S(1)} %get-tuple-element.67), channel_id=1, source_target_pairs={{0,1},{1,0},{2,3},{3,2},{4,5},{5,4},{6,7},{7,6},{8,9},{9,8},{10,11... | collective-permute-start | bytes 12296 | tf_op jit(solution)/shard_map/ppermute | solution.py:21
  31.2 5.0 %collective-permute-start.6 = (bf16[2,256,128]{2,1,0:T(8,128)(2,1)S(1)}, bf16[2,256,128]{2,1,0:T(8,128)(2,1)S(1)}, u32[]{:S(2)}, u32[]{:S(2)}) collective-permute-start(bf16[2,256,128]{2,1,0:T(8,128)(2,1)S(1)} %slice.79), channel_id=1, source_target_pairs={{0,8},{2,10},{4,12},{6,14},{8,0},{10,2},{12,4},{14,6},{16,24},{18,... | collective-permute-start | bytes 393224 | tf_op jit(solution)/shard_map/ppermute | solution.py:21
  32.0 5.0 %collective-permute-start.7 = (bf16[2,256,128]{2,1,0:T(8,128)(2,1)S(1)}, bf16[2,256,128]{2,1,0:T(8,128)(2,1)S(1)}, u32[]{:S(2)}, u32[]{:S(2)}) collective-permute-start(bf16[2,256,128]{2,1,0:T(8,128)(2,1)S(1)} %slice.78), channel_id=1, source_target_pairs={{0,4},{2,6},{4,0},{6,2},{8,12},{10,14},{12,8},{14,10},{16,20},{18,... | collective-permute-start | bytes 393224 | tf_op jit(solution)/shard_map/ppermute | solution.py:21
  32.9 3.0 %collective-permute-start.8 = (f32[40,512]{1,0:T(8,128)S(1)}, f32[40,512]{1,0:T(8,128)S(1)}, u32[]{:S(2)}, u32[]{:S(2)}) collective-permute-start(f32[40,512]{1,0:T(8,128)S(1)} %shard_map.123), channel_id=1, source_target_pairs={{0,2},{2,0},{4,6},{6,4},{8,10},{10,8},{12,14},{14,12},{16,18},{18,... | collective-permute-start | bytes 245768 | tf_op jit(solution)/shard_map/ppermute | solution.py:21
  32.9 8.6 %collective-permute-start.11 = (f32[4,32,128]{2,1,0:T(8,128)S(1)}, f32[4,32,128]{2,1,0:T(8,128)S(1)}, u32[]{:S(2)}, u32[]{:S(2)}) collective-permute-start(f32[4,32,128]{2,1,0:T(8,128)S(1)} %get-tuple-element.97), channel_id=1, source_target_pairs={{2,0},{4,2},{6,4},{8,6},{10,8},{12,10},{14,12},{16,14},{18,16},{20... | collective-permute-start | bytes 196616 | tf_op jit(solution)/shard_map/ppermute | solution.py:16
  34.2 7.3 %copy-start.4 = (bf16[512,512]{1,0:T(8,128)(2,1)S(1)}, bf16[512,512]{1,0:T(8,128)(2,1)}, u32[]{:S(2)}) copy-start(bf16[512,512]{1,0:T(8,128)(2,1)} %refs_4_.1) | copy-start | bytes 1572868
  37.1 9.2 %collective-permute-start.9 = (bf16[1,512,128]{2,1,0:T(8,128)(2,1)S(1)}, bf16[1,512,128]{2,1,0:T(8,128)(2,1)S(1)}, u32[]{:S(2)}, u32[]{:S(2)}) collective-permute-start(bf16[1,512,128]{2,1,0:T(8,128)(2,1)S(1)} %fusion.5), channel_id=1, source_target_pairs={{0,16},{2,18},{4,20},{6,22},{8,24},{10,26},{12,28},{14,30},{16,0},... | collective-permute-start | bytes 393224 | tf_op jit(solution)/shard_map/ppermute | solution.py:21
  40.3 4.5 %collective-permute-start.10 = (f32[40,512]{1,0:T(8,128)S(1)}, f32[40,512]{1,0:T(8,128)S(1)}, u32[]{:S(2)}, u32[]{:S(2)}) collective-permute-start(f32[40,512]{1,0:T(8,128)S(1)} %add.43), channel_id=1, source_target_pairs={{0,4},{2,6},{4,0},{6,2},{8,12},{10,14},{12,8},{14,10},{16,20},{18,... | collective-permute-start | bytes 245768 | tf_op jit(solution)/shard_map/ppermute | solution.py:21
  46.3 4.5 %collective-permute-start.12 = (f32[40,512]{1,0:T(8,128)S(1)}, f32[40,512]{1,0:T(8,128)S(1)}, u32[]{:S(2)}, u32[]{:S(2)}) collective-permute-start(f32[40,512]{1,0:T(8,128)S(1)} %add.44), channel_id=1, source_target_pairs={{0,8},{2,10},{4,12},{6,14},{8,0},{10,2},{12,4},{14,6},{16,24},{18,... | collective-permute-start | bytes 245768 | tf_op jit(solution)/shard_map/ppermute | solution.py:21
  50.9 6.3 %collective-permute-start.13 = (f32[40,512]{1,0:T(8,128)S(1)}, f32[40,512]{1,0:T(8,128)S(1)}, u32[]{:S(2)}, u32[]{:S(2)}) collective-permute-start(f32[40,512]{1,0:T(8,128)S(1)} %add.45), channel_id=1, source_target_pairs={{0,16},{2,18},{4,20},{6,22},{8,24},{10,26},{12,28},{14,30},{16,0},... | collective-permute-start | bytes 245768 | tf_op jit(solution)/shard_map/ppermute | solution.py:21
